TPU v7x, 32 devices: a whole 2x2x4 slice. The times are simulated.
32 devices in a mesh: grp: 2 (over y), sp: 4 (over z), tp: 4 (over x, core).
Axes of the slice: x: 2, y: 2, z: 4, core: 2. Of those that a mesh axis runs over, the one named last changes fastest.
Arguments:
- query_latent: bfloat16 [1024, 768], P(('grp', 'sp')), parts along dimension 0, may hold values from -6 to 6
- key_latent: bfloat16 [1024, 256], P(('grp', 'sp', 'tp')), parts along dimension 0, may hold values from -20 to 20
- rotary_key: bfloat16 [1024, 64], P(('grp', 'sp', 'tp')), parts along dimension 0, may hold values from -1000 to 1000
- query_gain: float32 [768], replicated, may hold values from 0.1 to 1.9
- latent_gain: float32 [256], replicated, may hold values from 0.1 to 1.9
- query_up: bfloat16 [768, 3072], P(None, 'tp'), may hold values from -0.21875 to 0.21875
- key_up: bfloat16 [256, 2048], P(None, 'tp'), may hold values from -0.375 to 0.375
- value_up: bfloat16 [256, 2048], P(None, 'tp'), may hold values from -0.375 to 0.375
- out_gain: float32 [2048], P('tp'), may hold values from 0.1 to 1.9
- out_weight: bfloat16 [2048, 4096], P('sp', 'tp'), may hold values from -0.125 to 0.125
Outputs:
- mixed: bfloat16 [1024, 4096], P(('grp', 'sp'), 'tp'), parts along dimension 0
There are 2 independent parts, one for each index of `grp`. A program takes and returns all parts, laid end to end along the dimension named above; an argument that names none is the same for every part. Nothing has to cross between parts.
All inputs are finite; a program needn't handle non-finite values.
Results may differ from a plain program's by a relative error of at most 0.02.
The roundings to bfloat16 on the way count: a program that leaves them out, or rounds other values in their place, can miss the bound.
Values may be sent and summed in bfloat16 or wider, within the bound.
A program may use at most 128 MiB of HBM per device.

v0:
```python
import functools

import jax
import jax.numpy as jnp
import numpy as np
from jax import lax
from jax.experimental import pallas as pl
from jax.experimental.pallas import tpu as pltpu
from jax.sharding import PartitionSpec as P

HEADS = 16
NOPE_DIM = 128
ROPE_DIM = 64
VALUE_DIM = 128
KVRANK = 256


norm_eps = 1e-06
rope_theta = 10000.0


def rms_scaled(inputs, gain_vec):
    widened = inputs.astype(jnp.float32)
    return (
        widened
        * lax.rsqrt(jnp.mean(widened * widened, axis=-1, keepdims=True) + norm_eps)
        * gain_vec
    )


def rotate_half(inputs, positions):
    half_width = inputs.shape[-1] // 2
    inverse = rope_theta ** (-jnp.arange(half_width, dtype=jnp.float32) / half_width)
    angles = positions[:, None] * inverse[None, :]
    if inputs.ndim == 3:
        angles = angles[:, None, :]
    cosine = jnp.cos(angles)
    sine = jnp.sin(angles)
    widened = inputs.astype(jnp.float32)
    first = widened[..., :half_width]
    second = widened[..., half_width:]
    return jnp.concatenate(
        [first * cosine - second * sine, second * cosine + first * sine], axis=-1
    )


def on_device(
    query_latent,
    key_latent,
    rotary_key,
    query_gain,
    latent_gain,
    query_up,
    key_up,
    value_up,
    out_gain,
    out_weight,
):
    block_rows = query_latent.shape[0]
    row_count = key_latent.shape[0]
    head_local = key_up.shape[1] // NOPE_DIM
    block_start = lax.axis_index("sp") * block_rows
    own_start = block_start + lax.axis_index("tp") * row_count
    score_scale = (NOPE_DIM + ROPE_DIM) ** (-0.5)
    normed = rms_scaled(query_latent, query_gain).astype(jnp.bfloat16)
    query_full = jnp.dot(normed, query_up, preferred_element_type=jnp.float32).astype(jnp.bfloat16)
    query_full = query_full.reshape(block_rows, head_local, NOPE_DIM + ROPE_DIM)
    query_positions = (block_start + jnp.arange(block_rows, dtype=jnp.int32)).astype(jnp.float32)
    query_plain = query_full[..., :NOPE_DIM]
    query_turned = rotate_half(query_full[..., NOPE_DIM:], query_positions).astype(jnp.bfloat16)
    latent_normed = rms_scaled(key_latent, latent_gain).astype(jnp.bfloat16)
    own_positions = (own_start + jnp.arange(row_count, dtype=jnp.int32)).astype(jnp.float32)
    key_turned = rotate_half(rotary_key, own_positions).astype(jnp.bfloat16)
    running_max = jnp.full((block_rows, head_local), -1e30, jnp.float32)
    running_sum = jnp.zeros((block_rows, head_local), jnp.float32)
    weighted = jnp.zeros((block_rows, head_local, KVRANK), jnp.float32)
    latents = lax.all_gather(latent_normed, ("sp", "tp"), axis=0, tiled=True)
    turned_keys = lax.all_gather(key_turned, ("sp", "tp"), axis=0, tiled=True)
    portion_rows = latents.shape[0]
    step_rows = min(portion_rows, 2048)
    for begin in range(0, portion_rows, step_rows):
        latent_part = latents[begin : begin + step_rows]
        turned_part = turned_keys[begin : begin + step_rows]
        key_plain = jnp.dot(latent_part, key_up, preferred_element_type=jnp.float32).astype(
            jnp.bfloat16
        )
        key_plain = key_plain.reshape(latent_part.shape[0], head_local, NOPE_DIM)
        scores = jnp.einsum(
            "qhd,khd->qhk", query_plain, key_plain, preferred_element_type=jnp.float32
        )
        scores = scores + jnp.einsum(
            "qhd,kd->qhk", query_turned, turned_part, preferred_element_type=jnp.float32
        )
        scores = scores * score_scale
        new_max = jnp.maximum(running_max, jnp.max(scores, axis=-1))
        rescale = jnp.exp(running_max - new_max)
        expo = jnp.exp(scores - new_max[..., None])
        running_sum = running_sum * rescale + jnp.sum(expo, axis=-1)
        weighted = weighted * rescale[..., None] + jnp.einsum(
            "qhk,kc->qhc",
            expo.astype(jnp.bfloat16),
            latent_part,
            preferred_element_type=jnp.float32,
        )
        running_max = new_max
    final_state = (running_max, running_sum, weighted)
    running_max, running_sum, weighted = final_state
    latent_mix = (weighted / running_sum[..., None]).astype(jnp.bfloat16)
    value_heads = value_up.reshape(KVRANK, head_local, VALUE_DIM)
    head_out = jnp.einsum(
        "qhc,chd->qhd", latent_mix, value_heads, preferred_element_type=jnp.float32
    ).astype(jnp.bfloat16)
    head_out = head_out.reshape(block_rows, head_local * VALUE_DIM)
    widened = head_out.astype(jnp.float32)
    square_part = jnp.sum(widened * widened, axis=1)
    gained = (widened * out_gain).astype(jnp.bfloat16)
    all_gained, square_parts = (
        lax.all_gather(gained, "tp", axis=1, tiled=True),
        lax.all_gather(square_part[:, None].astype(jnp.bfloat16), "tp", axis=1, tiled=True).astype(
            jnp.float32
        ),
    )
    all_squares = jnp.sum(square_parts, axis=1)
    own_sums = jnp.dot(
        all_gained,
        lax.all_gather(out_weight, "sp", axis=0, tiled=True),
        preferred_element_type=jnp.float32,
    )
    mean_square = all_squares / (HEADS * VALUE_DIM)
    return (own_sums * lax.rsqrt(mean_square + norm_eps)[:, None]).astype(jnp.bfloat16)


CHUNKS = 4
LANES = 128
MOST_STEPS = 8


def rope_table(tokens, width):
    half = width // 2
    inverse = np.float32(rope_theta) ** (-np.arange(half, dtype=np.float32) / np.float32(half))
    angles = np.arange(tokens, dtype=np.float32)[:, None] * inverse.astype(np.float32)[None, :]
    wide = angles.astype(np.float32).astype(np.float64)
    cosine, sine = np.cos(wide), np.sin(wide)
    return np.concatenate([cosine, cosine, -sine, sine], axis=1).astype(np.float32)


def turned(wide, table):
    width = wide.shape[-1]
    half = width // 2
    swapped = jnp.concatenate([wide[:, half:], wide[:, :half]], axis=1)
    return wide * table[:, :width] + swapped * table[:, width:]


def kernel(
    n_sp, n_tp,
    ql_hbm, kl, rk, qg_hbm, lg_hbm, og_hbm, table_hbm, qup, kup, vup, ow, out,
    ql, qg, lg, og, table,
    lat, rot, wbuf, qbuf, kbuf, vbuf, latn, kturn, qfull, qnorm, gall, acc,
    far_gained, far_out, far_in,
    local, s1_send, s1_recv, s2_send, s2_recv, g_send, g_recv,
    w_send, w_recv, y_send, y_recv, f_send, f_recv,
):
    z, t, g = lax.axis_index("sp"), lax.axis_index("tp"), lax.axis_index("grp")
    parity = lax.rem(g, 2)
    partner = g + 1 - 2 * parity
    block_rows = ql.shape[0]
    depth = ow.shape[0]
    half = depth // 2
    piece = half // CHUNKS
    heads = kup.shape[1] // NOPE_DIM
    cols = heads * VALUE_DIM
    head_width = NOPE_DIM + ROPE_DIM
    keys = n_sp * n_tp * kl.shape[0]

    near = pl.ds(pl.multiple_of(parity * half, half), half)
    far_half = pl.ds(pl.multiple_of((1 - parity) * half, half), half)
    loads = [
        pltpu.make_async_copy(src, dst, local.at[i])
        for i, (src, dst) in enumerate((
            (kl, lat.at[z, t]),
            (rk, rot.at[z, t]),
            (ow.at[near], wbuf.at[z, near]),
            (ql_hbm, ql),
            (qg_hbm, qg),
            (qup, qbuf),
            (lg_hbm, lg),
            (table_hbm, table),
            (kup, kbuf),
            (vup, vbuf),
            (og_hbm, og),
            (ow.at[far_half], wbuf.at[z, far_half]),
        ))
    ]
    for load in loads:
        load.start()

    barrier = pltpu.get_barrier_semaphore()
    for d in range(1, n_sp):
        pl.semaphore_signal(barrier, inc=1, device_id={"sp": lax.rem(z + d, n_sp)}, device_id_type=MESH)
    for d in range(1, n_tp):
        pl.semaphore_signal(barrier, inc=1, device_id={"tp": lax.rem(t + d, n_tp)}, device_id_type=MESH)
    pl.semaphore_signal(barrier, inc=1, device_id={"grp": partner}, device_id_type=MESH)
    pl.semaphore_wait(barrier, n_sp + n_tp - 1)

    def remote(src, dst, send, recv, target):
        return pltpu.make_async_remote_copy(
            src_ref=src, dst_ref=dst, send_sem=send, recv_sem=recv,
            device_id=target, device_id_type=MESH,
        )

    first = []
    for d in range(1, n_sp):
        target = {"sp": lax.rem(z + d, n_sp)}
        first.append(remote(lat.at[z, t], lat.at[z, t], s1_send.at[0, d], s1_recv.at[0, d], target))
        first.append(remote(rot.at[z, t], rot.at[z, t], s1_send.at[1, d], s1_recv.at[1, d], target))
    loads[0].wait()
    loads[1].wait()
    for copy in first:
        copy.start()

    def rows_of(b, c):
        return wbuf.at[b, pl.ds(pl.multiple_of(parity * half + c * piece, piece), piece)]

    def along(b, c, up):
        return remote(
            rows_of(b, c), rows_of(b, c), w_send.at[up, b, c], w_recv.at[b, c],
            {"sp": z + 1 if up else z - 1},
        )

    def far_rows_of(b, c):
        return wbuf.at[b, pl.ds(pl.multiple_of((1 - parity) * half + c * piece, piece), piece)]

    def along_far(c):
        return remote(
            far_rows_of(z, c), far_rows_of(z, c), y_send.at[z, c], y_recv.at[z, c],
            {"sp": jnp.where(z == 0, 1, n_sp - 2)},
        )

    def across(b, c):
        return remote(rows_of(b, c), rows_of(b, c), y_send.at[b, c], y_recv.at[b, c], {"grp": partner})

    has_up, has_down = z < n_sp - 1, z > 0
    reach = n_sp - 2
    at_edge = jnp.logical_or(z == 0, z == n_sp - 1)
    far = jnp.where(z == 0, n_sp - 1, 0)
    ask = remote(gall.at[far, :, pl.ds(0, cols)], far_gained, f_send.at[0], f_recv.at[0], {"sp": far})
    answer = remote(far_out, far_in, f_send.at[1], f_recv.at[1], {"sp": far})
    loads[2].wait()
    for c in range(CHUNKS):
        @pl.when(has_up)
        def _():
            along(z, c, 1).start()

        @pl.when(has_down)
        def _():
            along(z, c, 0).start()

    def event(k, c):
        @pl.when(z >= k)
        def _():
            b = z - k
            along(b, c, 1).wait_recv()

            if k < reach:
                @pl.when(has_up)
                def _():
                    along(b, c, 1).start()

            if k == 1:
                @pl.when(z > 1)
                def _():
                    across(b, c).start()
            else:
                across(b, c).start()

        @pl.when(z + k < n_sp)
        def _():
            b = z + k
            along(b, c, 0).wait_recv()

            if k < reach:
                @pl.when(has_down)
                def _():
                    along(b, c, 0).start()

            if k == 1:
                @pl.when(z < n_sp - 2)
                def _():
                    across(b, c).start()
            else:
                across(b, c).start()

    def block_product(b):
        acc[...] += jnp.dot(gall[b, :, :cols], wbuf[b], preferred_element_type=jnp.float32)

    def finish(k):
        @pl.when(z >= k)
        def _():
            for c in range(CHUNKS):
                across(z - k, c).wait_recv()
            block_product(z - k)

        @pl.when(z + k < n_sp)
        def _():
            for c in range(CHUNKS):
                across(z + k, c).wait_recv()
            block_product(z + k)

    second = []
    for d in range(1, n_tp):
        target = {"tp": lax.rem(t + d, n_tp)}
        second.append(remote(lat.at[:, t], lat.at[:, t], s2_send.at[0, d], s2_recv.at[0, d], target))
        second.append(remote(rot.at[:, t], rot.at[:, t], s2_send.at[1, d], s2_recv.at[1, d], target))

    def queries():
        loads[3].wait()
        loads[4].wait()
        loads[5].wait()
        wide = ql[...].astype(jnp.float32)
        mean = jnp.mean(wide * wide, axis=-1, keepdims=True)
        gain = jnp.concatenate([qg[i : i + 1] for i in range(qg.shape[0])], axis=1)
        qnorm[...] = (wide * lax.rsqrt(mean + norm_eps) * gain).astype(jnp.bfloat16)
        qfull[...] = jnp.dot(qnorm[...], qbuf[...], preferred_element_type=jnp.float32).astype(
            jnp.bfloat16
        )

    def far_halves():
        loads[11].wait()

        @pl.when(at_edge)
        def _():
            for c in range(CHUNKS):
                along_far(c).start()

    def spread():
        for copy in first:
            copy.wait_recv()
        for copy in second:
            copy.start()

    def latents():
        for load in loads[6:11]:
            load.wait()
        for copy in second:
            copy.wait_recv()
        wide = lat[...].reshape(keys, lat.shape[-1]).astype(jnp.float32)
        mean = jnp.mean(wide * wide, axis=-1, keepdims=True)
        latn[...] = (wide * lax.rsqrt(mean + norm_eps) * lg[...]).astype(jnp.bfloat16)
        spun = rot[...].reshape(keys, rot.shape[-1]).astype(jnp.float32)
        kturn[...] = turned(spun, table[...]).astype(jnp.bfloat16)

    transposed = (((1,), (1,)), ((), ()))

    def attend(h):
        start = h * head_width
        plain = qfull[:, start : start + NOPE_DIM]
        spun = qfull[:, start + NOPE_DIM : start + head_width].astype(jnp.float32)
        own = table[pl.ds(pl.multiple_of(z * block_rows, block_rows), block_rows), :]
        spun = turned(spun, own).astype(jnp.bfloat16)
        key_plain = jnp.dot(
            latn[...], kbuf[:, h * NOPE_DIM : (h + 1) * NOPE_DIM], preferred_element_type=jnp.float32
        ).astype(jnp.bfloat16)
        scores = lax.dot_general(plain, key_plain, transposed, preferred_element_type=jnp.float32)
        scores = scores + lax.dot_general(
            spun, kturn[...], transposed, preferred_element_type=jnp.float32
        )
        scores = scores * (head_width ** (-0.5))
        expo = jnp.exp(scores - jnp.max(scores, axis=-1, keepdims=True))
        total = jnp.sum(expo, axis=-1, keepdims=True)
        mix = jnp.dot(expo.astype(jnp.bfloat16), latn[...], preferred_element_type=jnp.float32)
        mix = (mix / total).astype(jnp.bfloat16)
        head_out = jnp.dot(
            mix, vbuf[:, h * VALUE_DIM : (h + 1) * VALUE_DIM], preferred_element_type=jnp.float32
        ).astype(jnp.bfloat16)
        wide = head_out.astype(jnp.float32)
        gained = wide * og[:, h * VALUE_DIM : (h + 1) * VALUE_DIM]
        gall[t, :, h * VALUE_DIM : (h + 1) * VALUE_DIM] = gained.astype(jnp.bfloat16)
        square = jnp.sum(wide * wide, axis=-1, keepdims=True)
        if h:
            square = square + acc[:, :1]
        acc[:, :VALUE_DIM] = jnp.broadcast_to(square, (block_rows, VALUE_DIM))
        if h == heads - 1:
            gall[t, :, cols:] = acc[:, :VALUE_DIM].astype(jnp.bfloat16)

    def head_part(h):
        width = VALUE_DIM if h < heads - 1 else 2 * VALUE_DIM
        return gall.at[t, :, pl.ds(h * VALUE_DIM, width)]

    shares = [
        [
            remote(head_part(h), head_part(h), g_send.at[h, d], g_recv.at[h, d], {"tp": lax.rem(t + d, n_tp)})
            for d in range(1, n_tp)
        ]
        for h in range(heads)
    ]

    def share(h):
        for copy in shares[h]:
            copy.start()

    def far_ask():
        for copy in sum(shares, []):
            copy.wait_recv()

        @pl.when(at_edge)
        def _():
            ask.start()

    def far_product():
        @pl.when(at_edge)
        def _():
            ask.wait_recv()
            far_out[...] = jnp.dot(
                far_gained[...], wbuf[z], preferred_element_type=jnp.float32
            ).astype(jnp.bfloat16)

    def own_product():
        acc[...] = jnp.zeros_like(acc)
        block_product(z)

    def far_answer():
        @pl.when(at_edge)
        def _():
            answer.start()

    work = [functools.partial(attend, h) for h in range(heads)]
    sends = [functools.partial(share, h) for h in range(heads)]
    middle = (heads + 1) // 2
    early = [call for pair in zip(work[:middle], [None] + sends[: middle - 1]) for call in pair if call]
    late = [
        call
        for pair in zip(work[middle:], sends[middle - 1 : heads - 1])
        for call in pair
    ]
    tasks = {
        0: [queries, far_halves, spread],
        1: [latents] + early,
        2: late,
        3: sends[heads - 1 :],
        4: [far_ask],
        7: [far_product, own_product, far_answer],
    }
    slot = 0
    for k in range(1, reach + 1):
        for c in range(CHUNKS):
            for task in tasks.pop(slot, []):
                task()
            event(k, c)
            slot += 1
    for left in sorted(tasks):
        for task in tasks[left]:
            task()
    for k in range(1, reach + 1):
        finish(k)

    @pl.when(at_edge)
    def _():
        answer.wait_recv()
        acc[...] += far_in[...].astype(jnp.float32)

    squares = gall[0, :, cols : cols + 1].astype(jnp.float32)
    for p in range(1, n_tp):
        squares = squares + gall[p, :, cols : cols + 1].astype(jnp.float32)
    scale = lax.rsqrt(squares / (n_tp * cols) + norm_eps)
    out[...] = (acc[...] * scale).astype(out.dtype)

    for copy in first + second + sum(shares, []):
        copy.wait_send()
    for c in range(CHUNKS):
        @pl.when(has_up)
        def _():
            along(z, c, 1).wait_send()

        @pl.when(has_down)
        def _():
            along(z, c, 0).wait_send()

    @pl.when(at_edge)
    def _():
        ask.wait_send()
        answer.wait_send()
        for c in range(CHUNKS):
            along_far(c).wait_send()

    for k in range(1, reach + 1):
        for c in range(CHUNKS):
            @pl.when(z >= max(k, 2))
            def _():
                across(z - k, c).wait_send()

            @pl.when(z + max(k, 2) < n_sp)
            def _():
                across(z + k, c).wait_send()

            if k < reach:
                @pl.when(jnp.logical_and(z >= k, has_up))
                def _():
                    along(z - k, c, 1).wait_send()

                @pl.when(jnp.logical_and(z + k < n_sp, has_down))
                def _():
                    along(z + k, c, 0).wait_send()


MESH = pl.DeviceIdType.MESH


def on_device_fused(
    n_sp, n_tp,
    query_latent, key_latent, rotary_key, query_gain, latent_gain,
    query_up, key_up, value_up, out_gain, out_weight,
):
    block_rows, row_count = query_latent.shape[0], key_latent.shape[0]
    rank, width = key_latent.shape[1], rotary_key.shape[1]
    keys = n_sp * n_tp * row_count
    depth, features = out_weight.shape
    cols = value_up.shape[1]
    vmem, bf16, dma = pltpu.VMEM, jnp.bfloat16, pltpu.SemaphoreType.DMA
    table = jnp.asarray(rope_table(keys, width))
    in_vmem = pl.BlockSpec(memory_space=pltpu.VMEM)
    in_hbm = pl.BlockSpec(memory_space=pl.ANY)
    return pl.pallas_call(
        functools.partial(kernel, n_sp, n_tp),
        out_shape=jax.ShapeDtypeStruct((block_rows, features), bf16),
        in_specs=[in_hbm] * 11,
        out_specs=in_vmem,
        scratch_shapes=[
            vmem(query_latent.shape, bf16),
            vmem((query_gain.shape[0] // LANES, LANES), jnp.float32),
            vmem((1, rank), jnp.float32),
            vmem((1, cols), jnp.float32),
            vmem(table.shape, jnp.float32),
            vmem((n_sp, n_tp, row_count, rank), bf16),
            vmem((n_sp, n_tp, row_count, width), bf16),
            vmem((n_sp, depth, features), bf16),
            vmem(query_up.shape, bf16),
            vmem(key_up.shape, bf16),
            vmem(value_up.shape, bf16),
            vmem((keys, rank), bf16),
            vmem((keys, width), bf16),
            vmem((block_rows, query_up.shape[1]), bf16),
            vmem(query_latent.shape, bf16),
            vmem((n_tp, block_rows, cols + VALUE_DIM), bf16),
            vmem((block_rows, features), jnp.float32),
            vmem((block_rows, cols), bf16),
            vmem((block_rows, features), bf16),
            vmem((block_rows, features), bf16),
            dma((12,)),
            dma((2, n_sp)),
            dma((2, n_sp)),
            dma((2, n_tp)),
            dma((2, n_tp)),
            dma((cols // VALUE_DIM, n_tp)),
            dma((cols // VALUE_DIM, n_tp)),
            dma((2, n_sp, CHUNKS)),
            dma((n_sp, CHUNKS)),
            dma((n_sp, CHUNKS)),
            dma((n_sp, CHUNKS)),
            dma((2,)),
            dma((2,)),
        ],
        compiler_params=pltpu.CompilerParams(
            collective_id=0, has_side_effects=True
        ),
    )(
        query_latent, key_latent, rotary_key, query_gain.reshape(-1, LANES), latent_gain[None], out_gain[None],
        table, query_up, key_up, value_up, out_weight,
    )


def fits_fused(mesh):
    n_grp, n_sp, n_tp = (mesh.shape[name] for name in ("grp", "sp", "tp"))
    return n_grp % 2 == 0 and 2 < n_sp <= MOST_STEPS and n_sp == n_tp


def solution(mesh):
    in_specs = (
        P(("grp", "sp"), None),
        P(("grp", "sp", "tp"), None),
        P(("grp", "sp", "tp"), None),
        P(),
        P(),
        P(None, "tp"),
        P(None, "tp"),
        P(None, "tp"),
        P("tp"),
        P("sp", "tp"),
    )
    out_specs = P(("grp", "sp"), "tp")
    step = on_device
    if fits_fused(mesh):
        step = functools.partial(on_device_fused, mesh.shape["sp"], mesh.shape["tp"])
    return jax.shard_map(
        step, mesh=mesh, in_specs=in_specs, out_specs=out_specs, check_vma=False
    )
```

profile of v0, /device:TPU:0, one launch (start us, length us, event | category | flops | bytes accessed | tf_op | source)
XLA Modules:
  0.0 46.3 jit_solution(14192569718374166874)
XLA Ops:
  0.0 44.6 %shard_map.109 = bf16[128,1024]{1,0:T(8,128)(2,1)} custom-call(bf16[128,768]{1,0:T(8,128)(2,1)} %ql_hbm.1, bf16[32,256]{1,0:T(8,128)(2,1)} %kl.1, bf16[32,64]{1,0:T(8,128)(2,1)} %rk.1, f32[6,128]{1,0:T(8,128)} %bitcast.3, f32[1,256]{1,0:T(1,128)} %bitcast.5, f32[1,512]{1,0:T(1,128)} %bitcast.4, f32[512,128]{1,0:T(8,128)} %constant.2.clone.table_hbm, ...), custom_call_target="tpu_custom_call" | custom-call | tf_op jit(solution)/shard_map/pallas_call | solution.py:522
  44.6 1.7 %copy.13 = bf16[128,1024]{1,0:T(8,128)(2,1)} copy(bf16[128,1024]{1,0:T(8,128)(2,1)} %shard_map.109) | data formatting | bytes 524288
where the time goes:
time: 46.4 us; the launch traced here: 46.3 us
  Pallas kernels  44.6 us (96%)
  local copies, waits for them, and re-layouts  1.67 us (4%)
    pallas_call x1, Pallas kernels, on_device_fused(): pl.pallas_call(functools.partial(kernel, n_sp, n_tp), out_shape=jax.Shape...  44.6 us
    unnamed x1, local copies, waits for them, and re-layouts  1.67 us

commit v1 on v0

v1 whole, which is shorter than its diff:
```python
import functools

import jax
import jax.numpy as jnp
import numpy as np
from jax import lax
from jax.experimental import pallas as pl
from jax.experimental.pallas import tpu as pltpu
from jax.sharding import PartitionSpec as P

HEADS = 16
NOPE_DIM = 128
ROPE_DIM = 64
VALUE_DIM = 128
KVRANK = 256


norm_eps = 1e-06
rope_theta = 10000.0


def rms_scaled(inputs, gain_vec):
    widened = inputs.astype(jnp.float32)
    return (
        widened
        * lax.rsqrt(jnp.mean(widened * widened, axis=-1, keepdims=True) + norm_eps)
        * gain_vec
    )


def rotate_half(inputs, positions):
    half_width = inputs.shape[-1] // 2
    inverse = rope_theta ** (-jnp.arange(half_width, dtype=jnp.float32) / half_width)
    angles = positions[:, None] * inverse[None, :]
    if inputs.ndim == 3:
        angles = angles[:, None, :]
    cosine = jnp.cos(angles)
    sine = jnp.sin(angles)
    widened = inputs.astype(jnp.float32)
    first = widened[..., :half_width]
    second = widened[..., half_width:]
    return jnp.concatenate(
        [first * cosine - second * sine, second * cosine + first * sine], axis=-1
    )


def on_device(
    query_latent,
    key_latent,
    rotary_key,
    query_gain,
    latent_gain,
    query_up,
    key_up,
    value_up,
    out_gain,
    out_weight,
):
    block_rows = query_latent.shape[0]
    row_count = key_latent.shape[0]
    head_local = key_up.shape[1] // NOPE_DIM
    block_start = lax.axis_index("sp") * block_rows
    own_start = block_start + lax.axis_index("tp") * row_count
    score_scale = (NOPE_DIM + ROPE_DIM) ** (-0.5)
    normed = rms_scaled(query_latent, query_gain).astype(jnp.bfloat16)
    query_full = jnp.dot(normed, query_up, preferred_element_type=jnp.float32).astype(jnp.bfloat16)
    query_full = query_full.reshape(block_rows, head_local, NOPE_DIM + ROPE_DIM)
    query_positions = (block_start + jnp.arange(block_rows, dtype=jnp.int32)).astype(jnp.float32)
    query_plain = query_full[..., :NOPE_DIM]
    query_turned = rotate_half(query_full[..., NOPE_DIM:], query_positions).astype(jnp.bfloat16)
    latent_normed = rms_scaled(key_latent, latent_gain).astype(jnp.bfloat16)
    own_positions = (own_start + jnp.arange(row_count, dtype=jnp.int32)).astype(jnp.float32)
    key_turned = rotate_half(rotary_key, own_positions).astype(jnp.bfloat16)
    running_max = jnp.full((block_rows, head_local), -1e30, jnp.float32)
    running_sum = jnp.zeros((block_rows, head_local), jnp.float32)
    weighted = jnp.zeros((block_rows, head_local, KVRANK), jnp.float32)
    latents = lax.all_gather(latent_normed, ("sp", "tp"), axis=0, tiled=True)
    turned_keys = lax.all_gather(key_turned, ("sp", "tp"), axis=0, tiled=True)
    portion_rows = latents.shape[0]
    step_rows = min(portion_rows, 2048)
    for begin in range(0, portion_rows, step_rows):
        latent_part = latents[begin : begin + step_rows]
        turned_part = turned_keys[begin : begin + step_rows]
        key_plain = jnp.dot(latent_part, key_up, preferred_element_type=jnp.float32).astype(
            jnp.bfloat16
        )
        key_plain = key_plain.reshape(latent_part.shape[0], head_local, NOPE_DIM)
        scores = jnp.einsum(
            "qhd,khd->qhk", query_plain, key_plain, preferred_element_type=jnp.float32
        )
        scores = scores + jnp.einsum(
            "qhd,kd->qhk", query_turned, turned_part, preferred_element_type=jnp.float32
        )
        scores = scores * score_scale
        new_max = jnp.maximum(running_max, jnp.max(scores, axis=-1))
        rescale = jnp.exp(running_max - new_max)
        expo = jnp.exp(scores - new_max[..., None])
        running_sum = running_sum * rescale + jnp.sum(expo, axis=-1)
        weighted = weighted * rescale[..., None] + jnp.einsum(
            "qhk,kc->qhc",
            expo.astype(jnp.bfloat16),
            latent_part,
            preferred_element_type=jnp.float32,
        )
        running_max = new_max
    final_state = (running_max, running_sum, weighted)
    running_max, running_sum, weighted = final_state
    latent_mix = (weighted / running_sum[..., None]).astype(jnp.bfloat16)
    value_heads = value_up.reshape(KVRANK, head_local, VALUE_DIM)
    head_out = jnp.einsum(
        "qhc,chd->qhd", latent_mix, value_heads, preferred_element_type=jnp.float32
    ).astype(jnp.bfloat16)
    head_out = head_out.reshape(block_rows, head_local * VALUE_DIM)
    widened = head_out.astype(jnp.float32)
    square_part = jnp.sum(widened * widened, axis=1)
    gained = (widened * out_gain).astype(jnp.bfloat16)
    all_gained, square_parts = (
        lax.all_gather(gained, "tp", axis=1, tiled=True),
        lax.all_gather(square_part[:, None].astype(jnp.bfloat16), "tp", axis=1, tiled=True).astype(
            jnp.float32
        ),
    )
    all_squares = jnp.sum(square_parts, axis=1)
    own_sums = jnp.dot(
        all_gained,
        lax.all_gather(out_weight, "sp", axis=0, tiled=True),
        preferred_element_type=jnp.float32,
    )
    mean_square = all_squares / (HEADS * VALUE_DIM)
    return (own_sums * lax.rsqrt(mean_square + norm_eps)[:, None]).astype(jnp.bfloat16)


LANES = 128
LINE = 4
TILES = 4
SPLIT = 2
CHUNKS = TILES * SPLIT


def rope_table(tokens, width):
    half = width // 2
    inverse = np.float32(rope_theta) ** (-np.arange(half, dtype=np.float32) / np.float32(half))
    angles = np.arange(tokens, dtype=np.float32)[:, None] * inverse.astype(np.float32)[None, :]
    wide = angles.astype(np.float32).astype(np.float64)
    cosine, sine = np.cos(wide), np.sin(wide)
    return np.concatenate([cosine, cosine, -sine, sine], axis=1).astype(np.float32)


def turned(wide, table):
    width = wide.shape[-1]
    half = width // 2
    swapped = jnp.concatenate([wide[:, half:], wide[:, :half]], axis=1)
    return wide * table[:, :width] + swapped * table[:, width:]


def kernel(
    n_sp, n_tp,
    ql_hbm, kl, rk, qg_hbm, lg_hbm, og_hbm, table_hbm, qup, kup, vup, ow, out_hbm,
    ql, qg, lg, og, table,
    lat, wbuf, qbuf, kbuf, vbuf, latn, kturn, qfull, qnorm, gall, squares, acc, far_acc,
    asked, far_out, far_in, out,
    local, w_local, o_local, l_send, l_recv, g_send, g_recv,
    w_send, w_recv, q_send, q_recv, f_send, f_recv,
):
    z, t, g = lax.axis_index("sp"), lax.axis_index("tp"), lax.axis_index("grp")
    parity = lax.rem(g, 2)
    partner = g + 1 - 2 * parity
    core = lax.rem(t, 2)
    sibling = t + 1 - 2 * core
    block_rows = ql.shape[0]
    depth = ow.shape[0]
    half = depth // 2
    piece = half // SPLIT
    tile = wbuf.shape[3]
    heads = kup.shape[1] // NOPE_DIM
    cols = heads * VALUE_DIM
    head_width = NOPE_DIM + ROPE_DIM
    rank = kl.shape[1]
    width = rk.shape[1]
    keys = n_sp * n_tp * kl.shape[0]

    lower = z < n_sp // 2
    toward = jnp.where(lower, 1, -1)
    centre = z + toward
    outer = z - toward
    beyond = centre + toward
    has_up, has_down = z < n_sp - 1, z > 0
    edge = jnp.logical_or(z == 0, z == n_sp - 1)
    inner = jnp.logical_not(edge)
    far_base = jnp.where(lower, n_tp // 2, 0)

    loads = [
        pltpu.make_async_copy(src, dst, local.at[i])
        for i, (src, dst) in enumerate((
            (kl, lat.at[z, t, :, pl.ds(0, rank)]),
            (rk, lat.at[z, t, :, pl.ds(rank, width)]),
            (ql_hbm, ql),
            (qg_hbm, qg),
            (qup, qbuf),
            (lg_hbm, lg),
            (table_hbm, table),
            (kup, kbuf),
            (vup, vbuf),
            (og_hbm, og),
        ))
    ]
    w_loads = [
        pltpu.make_async_copy(ow.at[:, pl.ds(f * tile, tile)], wbuf.at[z, f], w_local.at[f])
        for f in range(TILES)
    ]
    for load in loads[:2] + w_loads[:1] + loads[2:5] + w_loads[1:] + loads[5:]:
        load.start()

    barrier = pltpu.get_barrier_semaphore()

    @pl.when(has_up)
    def _():
        pl.semaphore_signal(barrier, inc=1, device_id={"sp": z + 1}, device_id_type=MESH)

    @pl.when(has_down)
    def _():
        pl.semaphore_signal(barrier, inc=1, device_id={"sp": z - 1}, device_id_type=MESH)

    pl.semaphore_signal(barrier, inc=1, device_id={"grp": partner}, device_id_type=MESH)
    for d in range(1, n_tp):
        pl.semaphore_signal(barrier, inc=1, device_id={"tp": lax.rem(t + d, n_tp)}, device_id_type=MESH)
    pl.semaphore_wait(barrier, n_tp + jnp.where(edge, 1, 2))

    def remote(src, dst, send, recv, target):
        return pltpu.make_async_remote_copy(
            src_ref=src, dst_ref=dst, send_sem=send, recv_sem=recv,
            device_id=target, device_id_type=MESH,
        )

    def part_along(b, up):
        return remote(
            lat.at[b, t], lat.at[b, t], l_send.at[b, up], l_recv.at[b, t], {"sp": z + 1 if up else z - 1}
        )

    def part_across(b, d):
        return remote(
            lat.at[b, t], lat.at[b, t], l_send.at[b, 1 + d], l_recv.at[b, t], {"tp": lax.rem(t + d, n_tp)}
        )

    def spread(b):
        for d in range(1, n_tp):
            part_across(b, d).start()

    def arrive(d):
        @pl.when(z >= d)
        def _():
            part_along(z - d, 1).wait_recv()

            @pl.when(has_up)
            def _():
                part_along(z - d, 1).start()

            spread(z - d)

        @pl.when(z + d < n_sp)
        def _():
            part_along(z + d, 0).wait_recv()

            @pl.when(has_down)
            def _():
                part_along(z + d, 0).start()

            spread(z + d)

    def rows_of(b, p, i):
        start = pl.multiple_of(p * half + (i % SPLIT) * piece, piece)
        return wbuf.at[b, i // SPLIT, pl.ds(start, piece)]

    def moved(kind, b, p, i, target):
        return remote(rows_of(b, p, i), rows_of(b, p, i), w_send.at[kind, i], w_recv.at[b, p, i], target)

    def inward(i):
        return moved(0, z, parity, i, {"sp": centre})

    def outward(i):
        return moved(1, z, parity, i, {"sp": outer})

    def passed(i):
        return moved(2, outer, parity, i, {"sp": centre})

    def inward_far(i):
        return moved(3, z, 1 - parity, i, {"sp": centre})

    def across(b, i):
        return moved(4, b, parity, i, {"grp": partner})

    def across_beyond(i):
        return moved(5, beyond, parity, i, {"grp": partner})

    def landed(b, p, i):
        moved(0, b, p, i, {"sp": centre}).wait_recv()

    def near(i):
        if i % SPLIT == 0:
            w_loads[i // SPLIT].wait()
        inward(i).start()

        @pl.when(inner)
        def _():
            outward(i).start()

    def near_far(i):
        @pl.when(edge)
        def _():
            inward_far(i).start()

    def first_hop(i):
        @pl.when(inner)
        def _():
            landed(outer, parity, i)
            passed(i).start()

        landed(centre, parity, i)
        across(centre, i).start()

    def second_hop(i):
        landed(beyond, parity, i)
        across_beyond(i).start()

    def queries():
        for load in loads[2:5]:
            load.wait()
        wide = ql[...].astype(jnp.float32)
        mean = jnp.mean(wide * wide, axis=-1, keepdims=True)
        gain = jnp.concatenate([qg[i : i + 1] for i in range(qg.shape[0])], axis=1)
        qnorm[...] = (wide * lax.rsqrt(mean + norm_eps) * gain).astype(jnp.bfloat16)
        qfull[...] = jnp.dot(qnorm[...], qbuf[...], preferred_element_type=jnp.float32).astype(
            jnp.bfloat16
        )

    def latents():
        for load in loads[5:]:
            load.wait()
        for b in range(n_sp):
            for d in range(1, n_tp):
                p = lax.rem(t + d, n_tp)
                remote(lat.at[b, p], lat.at[b, p], l_send.at[b, 1 + d], l_recv.at[b, p], {"tp": p}).wait_recv()
        whole = lat[...].reshape(keys, rank + width)
        wide = whole[:, :rank].astype(jnp.float32)
        mean = jnp.mean(wide * wide, axis=-1, keepdims=True)
        latn[...] = (wide * lax.rsqrt(mean + norm_eps) * lg[...]).astype(jnp.bfloat16)
        spun = whole[:, rank:].astype(jnp.float32)
        kturn[...] = turned(spun, table[...]).astype(jnp.bfloat16)

    transposed = (((1,), (1,)), ((), ()))

    def attend(h):
        start = h * head_width
        plain = qfull[:, start : start + NOPE_DIM]
        spun = qfull[:, start + NOPE_DIM : start + head_width].astype(jnp.float32)
        own = table[pl.ds(pl.multiple_of(z * block_rows, block_rows), block_rows), :]
        spun = turned(spun, own).astype(jnp.bfloat16)
        key_plain = jnp.dot(
            latn[...], kbuf[:, h * NOPE_DIM : (h + 1) * NOPE_DIM], preferred_element_type=jnp.float32
        ).astype(jnp.bfloat16)
        scores = lax.dot_general(plain, key_plain, transposed, preferred_element_type=jnp.float32)
        scores = scores + lax.dot_general(
            spun, kturn[...], transposed, preferred_element_type=jnp.float32
        )
        scores = scores * (head_width ** (-0.5))
        expo = jnp.exp(scores - jnp.max(scores, axis=-1, keepdims=True))
        total = jnp.sum(expo, axis=-1, keepdims=True)
        mix = jnp.dot(expo.astype(jnp.bfloat16), latn[...], preferred_element_type=jnp.float32)
        mix = (mix / total).astype(jnp.bfloat16)
        head_out = jnp.dot(
            mix, vbuf[:, h * VALUE_DIM : (h + 1) * VALUE_DIM], preferred_element_type=jnp.float32
        ).astype(jnp.bfloat16)
        wide = head_out.astype(jnp.float32)
        gained = wide * og[:, h * VALUE_DIM : (h + 1) * VALUE_DIM]
        gall[t, :, h * VALUE_DIM : (h + 1) * VALUE_DIM] = gained.astype(jnp.bfloat16)
        square = jnp.sum(wide * wide, axis=-1, keepdims=True)
        if h:
            square = square + squares[:, :1]
        squares[...] = jnp.broadcast_to(square, squares.shape)
        if h == heads - 1:
            gall[t, :, cols:] = squares[...].astype(jnp.bfloat16)

    def head_part(h):
        span = VALUE_DIM if h < heads - 1 else 2 * VALUE_DIM
        return gall.at[t, :, pl.ds(h * VALUE_DIM, span)]

    shares = [
        [
            remote(head_part(h), head_part(h), g_send.at[h, d], g_recv.at[h, d], {"tp": lax.rem(t + d, n_tp)})
            for d in range(1, n_tp)
        ]
        for h in range(heads)
    ]

    def share(h):
        for copy in shares[h]:
            copy.start()

    def gather(h):
        for copy in shares[h]:
            copy.wait_recv()

    ask_width = cols // 2

    def question(a):
        return pl.ds(a * ask_width, ask_width)

    def ask(a):
        return remote(
            gall.at[far_base + core, :, question(a)], asked.at[core, :, question(a)],
            q_send.at[0, a], q_recv.at[core, a], {"sp": centre},
        )

    def hand(a):
        return remote(
            asked.at[core, :, question(a)], asked.at[core, :, question(a)],
            q_send.at[1, a], q_recv.at[core, a], {"tp": sibling},
        )

    def heard(c, a):
        remote(
            asked.at[c, :, question(a)], asked.at[c, :, question(a)],
            q_send.at[1, a], q_recv.at[c, a], {"tp": sibling},
        ).wait_recv()

    def hand_on(a):
        heard(core, a)
        hand(a).start()

    def answer(f):
        return remote(far_out.at[f], far_in.at[f], f_send.at[f], f_recv.at[f], {"sp": outer})

    def part_of(p):
        return pl.ds(pl.multiple_of(p * half, half), half)

    def whole_dot(lhs, b, f):
        return jnp.dot(lhs, wbuf[b, f], preferred_element_type=jnp.float32)

    def gained_half(b, p, f):
        return jnp.dot(gall[b, :, part_of(p)], wbuf[b, f, part_of(p)], preferred_element_type=jnp.float32)

    def asked_half(b, p, f):
        return jnp.dot(
            asked[b - far_base, :, part_of(p)], wbuf[b, f, part_of(p)], preferred_element_type=jnp.float32
        )

    def stored(f):
        return pltpu.make_async_copy(out.at[f], out_hbm.at[:, pl.ds(f * tile, tile)], o_local.at[f])

    def put(f, total):
        square = gall[0, :, cols : cols + 1].astype(jnp.float32)
        for p in range(1, n_tp):
            square = square + gall[p, :, cols : cols + 1].astype(jnp.float32)
        scale = lax.rsqrt(square / (n_tp * cols) + norm_eps)
        out[f] = (total * scale).astype(out.dtype)
        stored(f).start()

    loads[0].wait()
    loads[1].wait()

    @pl.when(has_up)
    def _():
        part_along(z, 1).start()

    @pl.when(has_down)
    def _():
        part_along(z, 0).start()

    spread(z)
    near(0)
    near(1)
    queries()
    arrive(1)
    near(2)
    near(3)
    arrive(2)
    for i in range(4, CHUNKS):
        near(i)
    first_hop(0)
    first_hop(1)
    arrive(3)
    first_hop(2)
    latents()
    first_hop(3)
    attend(0)
    first_hop(4)
    near_far(0)
    attend(1)
    share(0)
    first_hop(5)
    first_hop(6)
    near_far(1)
    attend(2)
    share(1)
    first_hop(7)
    near_far(2)
    attend(3)
    share(2)

    @pl.when(inner)
    def _():
        second_hop(0)
        second_hop(1)

    share(3)
    gather(0)
    gather(1)

    @pl.when(edge)
    def _():
        ask(0).start()
        gather(2)
        gather(3)
        ask(1).start()
        for i in range(3, CHUNKS):
            inward_far(i).start()
        for f in range(TILES):
            acc[f] = whole_dot(gall[z, :, :cols], z, f)
        for f in range(TILES):
            for i in range(f * SPLIT, (f + 1) * SPLIT):
                landed(centre, 1 - parity, i)
            acc[f] += whole_dot(gall[centre, :, :cols], centre, f)
        for f in range(TILES):
            answer(f).wait_recv()
            put(f, acc[f] + far_in[f].astype(jnp.float32))

    @pl.when(inner)
    def _():
        second_hop(2)
        gather(2)
        gather(3)
        second_hop(3)
        hand_on(0)
        for f in range(TILES):
            acc[f] = whole_dot(gall[z, :, :cols], z, f)
        second_hop(4)
        for f in range(TILES):
            acc[f] += gained_half(outer, parity, f)
        second_hop(5)
        for i in range(CHUNKS):
            landed(centre, 1 - parity, i)
        for f in range(TILES):
            acc[f] += whole_dot(gall[centre, :, :cols], centre, f)
        hand_on(1)
        second_hop(6)
        for a in range(2):
            heard(1 - core, a)
        for f in range(TILES):
            far_acc[f] = whole_dot(asked[centre - far_base], centre, f)
        second_hop(7)
        for f in range(TILES):
            acc[f] += gained_half(beyond, parity, f)
            far_acc[f] += asked_half(beyond, parity, f)
            for i in range(f * SPLIT, (f + 1) * SPLIT):
                landed(beyond, 1 - parity, i)
            far_out[f] = (far_acc[f] + asked_half(beyond, 1 - parity, f)).astype(far_out.dtype)
            acc[f] += gained_half(beyond, 1 - parity, f)
            answer(f).start()
        for f in range(TILES):
            for i in range(f * SPLIT, (f + 1) * SPLIT):
                landed(outer, 1 - parity, i)
            put(f, acc[f] + gained_half(outer, 1 - parity, f))

    for b in range(n_sp):
        for d in range(1, n_tp):
            part_across(b, d).wait_send()

        @pl.when(jnp.logical_and(z >= b, has_up))
        def _():
            part_along(b, 1).wait_send()

        @pl.when(jnp.logical_and(z <= b, has_down))
        def _():
            part_along(b, 0).wait_send()

    for copy in sum(shares, []):
        copy.wait_send()
    for i in range(CHUNKS):
        inward(i).wait_send()
        across(centre, i).wait_send()

    @pl.when(edge)
    def _():
        for i in range(CHUNKS):
            inward_far(i).wait_send()
        for a in range(2):
            ask(a).wait_send()

    @pl.when(inner)
    def _():
        for i in range(CHUNKS):
            outward(i).wait_send()
            passed(i).wait_send()
            across_beyond(i).wait_send()
        for a in range(2):
            hand(a).wait_send()
        for f in range(TILES):
            answer(f).wait_send()

    for f in range(TILES):
        stored(f).wait()


MESH = pl.DeviceIdType.MESH


def on_device_fused(
    n_sp, n_tp,
    query_latent, key_latent, rotary_key, query_gain, latent_gain,
    query_up, key_up, value_up, out_gain, out_weight,
):
    block_rows, row_count = query_latent.shape[0], key_latent.shape[0]
    rank, width = key_latent.shape[1], rotary_key.shape[1]
    keys = n_sp * n_tp * row_count
    depth, features = out_weight.shape
    cols = value_up.shape[1]
    vmem, bf16, dma = pltpu.VMEM, jnp.bfloat16, pltpu.SemaphoreType.DMA
    table = jnp.asarray(rope_table(keys, width))
    tiled = (TILES, block_rows, features // TILES)
    in_hbm = pl.BlockSpec(memory_space=pl.ANY)
    return pl.pallas_call(
        functools.partial(kernel, n_sp, n_tp),
        out_shape=jax.ShapeDtypeStruct((block_rows, features), bf16),
        in_specs=[in_hbm] * 11,
        out_specs=in_hbm,
        scratch_shapes=[
            vmem(query_latent.shape, bf16),
            vmem((query_gain.shape[0] // LANES, LANES), jnp.float32),
            vmem((1, rank), jnp.float32),
            vmem((1, cols), jnp.float32),
            vmem(table.shape, jnp.float32),
            vmem((n_sp, n_tp, row_count, rank + width), bf16),
            vmem((n_sp, TILES, depth, features // TILES), bf16),
            vmem(query_up.shape, bf16),
            vmem(key_up.shape, bf16),
            vmem(value_up.shape, bf16),
            vmem((keys, rank), bf16),
            vmem((keys, width), bf16),
            vmem((block_rows, query_up.shape[1]), bf16),
            vmem(query_latent.shape, bf16),
            vmem((n_tp, block_rows, cols + VALUE_DIM), bf16),
            vmem((block_rows, VALUE_DIM), jnp.float32),
            vmem(tiled, jnp.float32),
            vmem(tiled, jnp.float32),
            vmem((n_tp // 2, block_rows, cols), bf16),
            vmem(tiled, bf16),
            vmem(tiled, bf16),
            vmem(tiled, bf16),
            dma((10,)),
            dma((TILES,)),
            dma((TILES,)),
            dma((n_sp, n_tp + 1)),
            dma((n_sp, n_tp)),
            dma((cols // VALUE_DIM, n_tp)),
            dma((cols // VALUE_DIM, n_tp)),
            dma((6, CHUNKS)),
            dma((n_sp, 2, CHUNKS)),
            dma((2, 2)),
            dma((n_tp // 2, 2)),
            dma((TILES,)),
            dma((TILES,)),
        ],
        compiler_params=pltpu.CompilerParams(
            collective_id=0, has_side_effects=True
        ),
    )(
        query_latent, key_latent, rotary_key, query_gain.reshape(-1, LANES), latent_gain[None], out_gain[None],
        table, query_up, key_up, value_up, out_weight,
    )


def fits_fused(mesh):
    n_grp, n_sp, n_tp = (mesh.shape[name] for name in ("grp", "sp", "tp"))
    return n_grp % 2 == 0 and n_sp == LINE and n_sp == n_tp


def solution(mesh):
    in_specs = (
        P(("grp", "sp"), None),
        P(("grp", "sp", "tp"), None),
        P(("grp", "sp", "tp"), None),
        P(),
        P(),
        P(None, "tp"),
        P(None, "tp"),
        P(None, "tp"),
        P("tp"),
        P("sp", "tp"),
    )
    out_specs = P(("grp", "sp"), "tp")
    step = on_device
    if fits_fused(mesh):
        step = functools.partial(on_device_fused, mesh.shape["sp"], mesh.shape["tp"])
    return jax.shard_map(
        step, mesh=mesh, in_specs=in_specs, out_specs=out_specs, check_vma=False
    )
```

time: 46.4 us -> 44.5 us (0.959)
  Pallas kernels: 44.6 us -> 42.7 us
    pallas_call x1, Pallas kernels: 44.6 us -> 42.7 us  [on_device_fused(): pl.pallas_call(functools.partial(kernel, n_sp, n_tp), out_shape=jax.Shape...]
where the time goes in v1:
time: 44.5 us; the launch traced here: 44.4 us
  Pallas kernels  42.7 us (96%)
  local copies, waits for them, and re-layouts  1.67 us (4%)
    pallas_call x1, Pallas kernels, on_device_fused(): pl.pallas_call(functools.partial(kernel, n_sp, n_tp), out_shape=jax.Shape...  42.7 us
    unnamed x1, local copies, waits for them, and re-layouts  1.67 us

profile of v1, /device:TPU:0, one launch (start us, length us, event | category | flops | bytes accessed | tf_op | source)
XLA Modules:
  0.0 44.4 jit_solution(15105215117247335637)
XLA Ops:
  0.0 42.7 %shard_map.109 = bf16[128,1024]{1,0:T(8,128)(2,1)} custom-call(bf16[128,768]{1,0:T(8,128)(2,1)} %ql_hbm.1, bf16[32,256]{1,0:T(8,128)(2,1)} %kl.1, bf16[32,64]{1,0:T(8,128)(2,1)} %rk.1, f32[6,128]{1,0:T(8,128)} %bitcast.3, f32[1,256]{1,0:T(1,128)} %bitcast.5, f32[1,512]{1,0:T(1,128)} %bitcast.4, f32[512,128]{1,0:T(8,128)} %constant.2.clone.table_hbm, ...), custom_call_target="tpu_custom_call" | custom-call | tf_op jit(solution)/shard_map/pallas_call | solution.py:621
  42.7 1.7 %copy.13 = bf16[128,1024]{1,0:T(8,128)(2,1)} copy(bf16[128,1024]{1,0:T(8,128)(2,1)} %shard_map.109) | data formatting | bytes 524288

commit v2 on v1

--- a/solution.py
+++ b/solution.py
@@ -132,9 +132,10 @@
 
 LANES = 128
 LINE = 4
-TILES = 4
+TILES = 8
 SPLIT = 2
 CHUNKS = TILES * SPLIT
+TAIL = 3
 
 
 def rope_table(tokens, width):
@@ -157,10 +158,10 @@
     n_sp, n_tp,
     ql_hbm, kl, rk, qg_hbm, lg_hbm, og_hbm, table_hbm, qup, kup, vup, ow, out_hbm,
     ql, qg, lg, og, table,
-    lat, wbuf, qbuf, kbuf, vbuf, latn, kturn, qfull, qnorm, gall, squares, acc, far_acc,
-    asked, far_out, far_in, out,
+    lat, wbuf, qbuf, kbuf, vbuf, latn, kturn, qfull, qnorm, gall, squares, acc, asked,
+    far_out, far_in, out,
     local, w_local, o_local, l_send, l_recv, g_send, g_recv,
-    w_send, w_recv, q_send, q_recv, f_send, f_recv,
+    w_send, w_recv, q_send, q_recv, h_send, h_recv, f_send, f_recv,
 ):
     z, t, g = lax.axis_index("sp"), lax.axis_index("tp"), lax.axis_index("grp")
     parity = lax.rem(g, 2)
@@ -188,6 +189,7 @@
     edge = jnp.logical_or(z == 0, z == n_sp - 1)
     inner = jnp.logical_not(edge)
     far_base = jnp.where(lower, n_tp // 2, 0)
+    far_order = [*range(CHUNKS - TAIL, CHUNKS), *range(CHUNKS - TAIL)]
 
     loads = [
         pltpu.make_async_copy(src, dst, local.at[i])
@@ -286,6 +288,9 @@
     def inward_far(i):
         return moved(3, z, 1 - parity, i, {"sp": centre})
 
+    def passed_far(i):
+        return moved(6, outer, 1 - parity, i, {"sp": centre})
+
     def across(b, i):
         return moved(4, b, parity, i, {"grp": partner})
 
@@ -300,27 +305,44 @@
             w_loads[i // SPLIT].wait()
         inward(i).start()
 
+    def near_out(i):
         @pl.when(inner)
         def _():
             outward(i).start()
 
-    def near_far(i):
+    def near_far(some):
         @pl.when(edge)
         def _():
-            inward_far(i).start()
-
-    def first_hop(i):
-        @pl.when(inner)
-        def _():
-            landed(outer, parity, i)
-            passed(i).start()
-
+            for i in some:
+                inward_far(i).start()
+
+    def to_partner(i):
         landed(centre, parity, i)
         across(centre, i).start()
 
+    def inner_hop(some):
+        @pl.when(inner)
+        def _():
+            for i in some:
+                landed(outer, parity, i)
+                passed(i).start()
+                to_partner(i)
+
+    def edge_hop(some):
+        @pl.when(edge)
+        def _():
+            for i in some:
+                to_partner(i)
+
     def second_hop(i):
         landed(beyond, parity, i)
-        across_beyond(i).start()
+        if i < CHUNKS - TAIL:
+            across_beyond(i).start()
+
+    def first_hop_far():
+        for i in range(CHUNKS - TAIL, CHUNKS):
+            landed(outer, 1 - parity, i)
+            passed_far(i).start()
 
     def queries():
         for load in loads[2:5]:
@@ -380,52 +402,61 @@
         if h == heads - 1:
             gall[t, :, cols:] = squares[...].astype(jnp.bfloat16)
 
-    def head_part(h):
-        span = VALUE_DIM if h < heads - 1 else 2 * VALUE_DIM
-        return gall.at[t, :, pl.ds(h * VALUE_DIM, span)]
-
-    shares = [
-        [
-            remote(head_part(h), head_part(h), g_send.at[h, d], g_recv.at[h, d], {"tp": lax.rem(t + d, n_tp)})
-            for d in range(1, n_tp)
-        ]
-        for h in range(heads)
-    ]
+    def is_near(p):
+        return jnp.logical_or(p < far_base, p >= far_base + n_tp // 2)
+
+    def share_copy(h, d):
+        part = gall.at[t, :, pl.ds(h * VALUE_DIM, VALUE_DIM)]
+        return remote(part, part, g_send.at[h, d], g_recv.at[h, d], {"tp": lax.rem(t + d, n_tp)})
+
+    def each_share(h, d, p, act):
+        @pl.when(jnp.logical_or(inner, is_near(p)) if h < heads else True)
+        def _():
+            act(share_copy(h, d))
 
     def share(h):
-        for copy in shares[h]:
-            copy.start()
+        for d in range(1, n_tp):
+            each_share(h, d, t, lambda copy: copy.start())
+        if h < heads:
+            @pl.when(asks)
+            def _():
+                for kind in range(2):
+                    ask(h, kind).start()
+
+    def sent(h):
+        for d in range(1, n_tp):
+            each_share(h, d, t, lambda copy: copy.wait_send())
 
     def gather(h):
-        for copy in shares[h]:
-            copy.wait_recv()
-
-    ask_width = cols // 2
-
-    def question(a):
-        return pl.ds(a * ask_width, ask_width)
-
-    def ask(a):
+        for d in range(1, n_tp):
+            each_share(h, d, lax.rem(t + n_tp - d, n_tp), lambda copy: copy.wait_recv())
+
+    asks = jnp.logical_and(edge, jnp.logical_not(is_near(t)))
+    opposite = lax.rem(t + n_tp // 2, n_tp)
+
+    def head_of(h):
+        return pl.ds(h * VALUE_DIM, VALUE_DIM)
+
+    def ask(h, kind):
         return remote(
-            gall.at[far_base + core, :, question(a)], asked.at[core, :, question(a)],
-            q_send.at[0, a], q_recv.at[core, a], {"sp": centre},
-        )
-
-    def hand(a):
-        return remote(
-            asked.at[core, :, question(a)], asked.at[core, :, question(a)],
-            q_send.at[1, a], q_recv.at[core, a], {"tp": sibling},
-        )
-
-    def heard(c, a):
-        remote(
-            asked.at[c, :, question(a)], asked.at[c, :, question(a)],
-            q_send.at[1, a], q_recv.at[c, a], {"tp": sibling},
-        ).wait_recv()
+            gall.at[t, :, head_of(h)], asked.at[core, :, head_of(h)],
+            q_send.at[kind, h], q_recv.at[h], {"sp": centre, "tp": opposite} if kind else {"sp": centre},
+        )
+
+    def pair_of(a):
+        return pl.ds(a * (cols // 2), cols // 2)
+
+    def hand(c, a):
+        part = asked.at[c, :, pair_of(a)]
+        return remote(part, part, h_send.at[a], h_recv.at[a], {"tp": sibling})
 
     def hand_on(a):
-        heard(core, a)
-        hand(a).start()
+        for h in range(a * heads // 2, (a + 1) * heads // 2):
+            ask(h, 0).wait_recv()
+        hand(core, a).start()
+
+    def heard(a):
+        hand(1 - core, a).wait_recv()
 
     def answer(f):
         return remote(far_out.at[f], far_in.at[f], f_send.at[f], f_recv.at[f], {"sp": outer})
@@ -433,27 +464,42 @@
     def part_of(p):
         return pl.ds(pl.multiple_of(p * half, half), half)
 
-    def whole_dot(lhs, b, f):
-        return jnp.dot(lhs, wbuf[b, f], preferred_element_type=jnp.float32)
-
-    def gained_half(b, p, f):
-        return jnp.dot(gall[b, :, part_of(p)], wbuf[b, f, part_of(p)], preferred_element_type=jnp.float32)
-
-    def asked_half(b, p, f):
-        return jnp.dot(
-            asked[b - far_base, :, part_of(p)], wbuf[b, f, part_of(p)], preferred_element_type=jnp.float32
-        )
+    def wide_of(b, some):
+        return jnp.concatenate([wbuf[b, f] for f in some], axis=1)
+
+    def dot(lhs, b, some):
+        return jnp.dot(lhs, wide_of(b, some), preferred_element_type=jnp.float32)
+
+    def gained(b):
+        return gall[b, :, :cols]
+
+    def keep(some, total, fresh=False):
+        for n, f in enumerate(some):
+            part = total[:, n * tile : (n + 1) * tile]
+            acc[f] = part if fresh else acc[f] + part
 
     def stored(f):
         return pltpu.make_async_copy(out.at[f], out_hbm.at[:, pl.ds(f * tile, tile)], o_local.at[f])
 
-    def put(f, total):
+    def set_scale():
         square = gall[0, :, cols : cols + 1].astype(jnp.float32)
         for p in range(1, n_tp):
             square = square + gall[p, :, cols : cols + 1].astype(jnp.float32)
-        scale = lax.rsqrt(square / (n_tp * cols) + norm_eps)
-        out[f] = (total * scale).astype(out.dtype)
+        squares[...] = jnp.broadcast_to(lax.rsqrt(square / (n_tp * cols) + norm_eps), squares.shape)
+
+    def put(f, total):
+        out[f] = (total * squares[...]).astype(out.dtype)
         stored(f).start()
+
+    def run(call, some):
+        for i in some:
+            call(i)
+
+    tiles = range(TILES)
+    pairs = [(f, f + 1) for f in range(0, TILES, 2)]
+
+    def chunks_of(some):
+        return range(some[0] * SPLIT, (some[-1] + 1) * SPLIT)
 
     loads[0].wait()
     loads[1].wait()
@@ -467,99 +513,101 @@
         part_along(z, 0).start()
 
     spread(z)
-    near(0)
-    near(1)
+    run(near, range(5))
     queries()
     arrive(1)
-    near(2)
-    near(3)
+    run(near, range(5, CHUNKS))
+    run(near_out, range(4))
     arrive(2)
-    for i in range(4, CHUNKS):
-        near(i)
-    first_hop(0)
-    first_hop(1)
+    run(near_out, range(4, CHUNKS))
+    inner_hop(range(4))
     arrive(3)
-    first_hop(2)
+    inner_hop(range(4, 6))
+    near_far(far_order[:4])
     latents()
-    first_hop(3)
+    inner_hop(range(6, 8))
     attend(0)
-    first_hop(4)
-    near_far(0)
+    inner_hop(range(8, 10))
+    edge_hop(range(6))
+    near_far(far_order[4:8])
     attend(1)
     share(0)
-    first_hop(5)
-    first_hop(6)
-    near_far(1)
+    inner_hop(range(10, 12))
+    edge_hop(range(6, 8))
     attend(2)
     share(1)
-    first_hop(7)
-    near_far(2)
+    inner_hop(range(12, 14))
+    edge_hop(range(8, 9))
+    near_far(far_order[8:12])
     attend(3)
     share(2)
+    inner_hop(range(14, CHUNKS))
+    edge_hop(range(9, 11))
 
     @pl.when(inner)
     def _():
-        second_hop(0)
-        second_hop(1)
+        first_hop_far()
+        run(second_hop, range(2))
 
     share(3)
-    gather(0)
-    gather(1)
+    share(heads)
 
     @pl.when(edge)
     def _():
-        ask(0).start()
-        gather(2)
-        gather(3)
-        ask(1).start()
-        for i in range(3, CHUNKS):
+        run(to_partner, range(11, 13))
+        for i in far_order[12:]:
             inward_far(i).start()
-        for f in range(TILES):
-            acc[f] = whole_dot(gall[z, :, :cols], z, f)
-        for f in range(TILES):
-            for i in range(f * SPLIT, (f + 1) * SPLIT):
+        run(to_partner, range(13, CHUNKS))
+        for h in range(heads + 1):
+            gather(h)
+        set_scale()
+        for some in pairs:
+            keep(some, dot(gained(z), z, some), fresh=True)
+        for some in pairs:
+            for i in chunks_of(some):
                 landed(centre, 1 - parity, i)
-            acc[f] += whole_dot(gall[centre, :, :cols], centre, f)
-        for f in range(TILES):
+            keep(some, dot(gained(centre), centre, some))
+        for f in tiles:
             answer(f).wait_recv()
             put(f, acc[f] + far_in[f].astype(jnp.float32))
 
     @pl.when(inner)
     def _():
-        second_hop(2)
-        gather(2)
-        gather(3)
-        second_hop(3)
+        run(second_hop, range(2, 7))
+        for h in range(heads + 1):
+            gather(h)
+        run(second_hop, range(7, 8))
+        set_scale()
+        for some in pairs:
+            keep(some, dot(gained(z), z, some), fresh=True)
         hand_on(0)
-        for f in range(TILES):
-            acc[f] = whole_dot(gall[z, :, :cols], z, f)
-        second_hop(4)
-        for f in range(TILES):
-            acc[f] += gained_half(outer, parity, f)
-        second_hop(5)
+        run(second_hop, range(8, 9))
         for i in range(CHUNKS):
             landed(centre, 1 - parity, i)
-        for f in range(TILES):
-            acc[f] += whole_dot(gall[centre, :, :cols], centre, f)
+        for some in pairs:
+            keep(some, dot(gained(centre), centre, some))
         hand_on(1)
-        second_hop(6)
+        run(second_hop, range(9, 11))
         for a in range(2):
-            heard(1 - core, a)
-        for f in range(TILES):
-            far_acc[f] = whole_dot(asked[centre - far_base], centre, f)
-        second_hop(7)
-        for f in range(TILES):
-            acc[f] += gained_half(beyond, parity, f)
-            far_acc[f] += asked_half(beyond, parity, f)
-            for i in range(f * SPLIT, (f + 1) * SPLIT):
+            heard(a)
+        for some in pairs[:-1] + [(f,) for f in pairs[-1]]:
+            run(second_hop, [i for i in chunks_of(some) if i >= 11])
+            for i in chunks_of(some):
                 landed(beyond, 1 - parity, i)
-            far_out[f] = (far_acc[f] + asked_half(beyond, 1 - parity, f)).astype(far_out.dtype)
-            acc[f] += gained_half(beyond, 1 - parity, f)
-            answer(f).start()
-        for f in range(TILES):
-            for i in range(f * SPLIT, (f + 1) * SPLIT):
-                landed(outer, 1 - parity, i)
-            put(f, acc[f] + gained_half(outer, 1 - parity, f))
+            both = jnp.concatenate([gained(beyond), asked[beyond - far_base]], axis=0)
+            both = dot(both, beyond, some)
+            far = both[block_rows:] + dot(asked[centre - far_base], centre, some)
+            for n, f in enumerate(some):
+                far_out[f] = far[:, n * tile : (n + 1) * tile].astype(far_out.dtype)
+            for f in some:
+                answer(f).start()
+            keep(some, both[:block_rows])
+        for i in range(CHUNKS - TAIL):
+            landed(outer, 1 - parity, i)
+        for some in pairs:
+            total = dot(gained(outer), outer, some)
+            for n, f in enumerate(some):
+                put(f, acc[f] + total[:, n * tile : (n + 1) * tile])
 
     for b in range(n_sp):
         for d in range(1, n_tp):
@@ -573,8 +621,8 @@
         def _():
             part_along(b, 0).wait_send()
 
-    for copy in sum(shares, []):
-        copy.wait_send()
+    for h in range(heads + 1):
+        sent(h)
     for i in range(CHUNKS):
         inward(i).wait_send()
         across(centre, i).wait_send()
@@ -583,17 +631,24 @@
     def _():
         for i in range(CHUNKS):
             inward_far(i).wait_send()
-        for a in range(2):
-            ask(a).wait_send()
+
+    @pl.when(asks)
+    def _():
+        for h in range(heads):
+            for kind in range(2):
+                ask(h, kind).wait_send()
 
     @pl.when(inner)
     def _():
         for i in range(CHUNKS):
             outward(i).wait_send()
             passed(i).wait_send()
-            across_beyond(i).wait_send()
+            if i < CHUNKS - TAIL:
+                across_beyond(i).wait_send()
+            else:
+                passed_far(i).wait_send()
         for a in range(2):
-            hand(a).wait_send()
+            hand(core, a).wait_send()
         for f in range(TILES):
             answer(f).wait_send()
 
@@ -641,7 +696,6 @@
             vmem((n_tp, block_rows, cols + VALUE_DIM), bf16),
             vmem((block_rows, VALUE_DIM), jnp.float32),
             vmem(tiled, jnp.float32),
-            vmem(tiled, jnp.float32),
             vmem((n_tp // 2, block_rows, cols), bf16),
             vmem(tiled, bf16),
             vmem(tiled, bf16),
@@ -651,12 +705,14 @@
             dma((TILES,)),
             dma((n_sp, n_tp + 1)),
             dma((n_sp, n_tp)),
-            dma((cols // VALUE_DIM, n_tp)),
-            dma((cols // VALUE_DIM, n_tp)),
-            dma((6, CHUNKS)),
+            dma((cols // VALUE_DIM + 1, n_tp)),
+            dma((cols // VALUE_DIM + 1, n_tp)),
+            dma((7, CHUNKS)),
             dma((n_sp, 2, CHUNKS)),
-            dma((2, 2)),
-            dma((n_tp // 2, 2)),
+            dma((2, cols // VALUE_DIM)),
+            dma((cols // VALUE_DIM,)),
+            dma((2,)),
+            dma((2,)),
             dma((TILES,)),
             dma((TILES,)),
         ],

time: 44.5 us -> 49.2 us (1.11)
  Pallas kernels: 42.7 us -> 47.4 us
    pallas_call x1, Pallas kernels: 42.7 us -> 47.4 us  [on_device_fused(): pl.pallas_call(functools.partial(kernel, n_sp, n_tp), out_shape=jax.Shape...]
where the time goes in v2:
time: 49.2 us; the launch traced here: 49.1 us
  Pallas kernels  47.4 us (96%)
  local copies, waits for them, and re-layouts  1.67 us (3%)
    pallas_call x1, Pallas kernels, on_device_fused(): pl.pallas_call(functools.partial(kernel, n_sp, n_tp), out_shape=jax.Shape...  47.4 us
    unnamed x1, local copies, waits for them, and re-layouts  1.67 us

profile of v2, /device:TPU:0, one launch (start us, length us, event | category | flops | bytes accessed | tf_op | source)
XLA Modules:
  0.0 49.1 jit_solution(3709770134378423511)
XLA Ops:
  0.0 47.4 %shard_map.109 = bf16[128,1024]{1,0:T(8,128)(2,1)} custom-call(bf16[128,768]{1,0:T(8,128)(2,1)} %ql_hbm.1, bf16[32,256]{1,0:T(8,128)(2,1)} %kl.1, bf16[32,64]{1,0:T(8,128)(2,1)} %rk.1, f32[6,128]{1,0:T(8,128)} %bitcast.3, f32[1,256]{1,0:T(1,128)} %bitcast.5, f32[1,512]{1,0:T(1,128)} %bitcast.4, f32[512,128]{1,0:T(8,128)} %constant.2.clone.table_hbm, ...), custom_call_target="tpu_custom_call" | custom-call | tf_op jit(solution)/shard_map/pallas_call | solution.py:676
  47.4 1.7 %copy.13 = bf16[128,1024]{1,0:T(8,128)(2,1)} copy(bf16[128,1024]{1,0:T(8,128)(2,1)} %shard_map.109) | data formatting | bytes 524288

commit v3 on v2

--- a/solution.py
+++ b/solution.py
@@ -133,9 +133,6 @@
 LANES = 128
 LINE = 4
 TILES = 8
-SPLIT = 2
-CHUNKS = TILES * SPLIT
-TAIL = 3
 
 
 def rope_table(tokens, width):
@@ -157,11 +154,12 @@
 def kernel(
     n_sp, n_tp,
     ql_hbm, kl, rk, qg_hbm, lg_hbm, og_hbm, table_hbm, qup, kup, vup, ow, out_hbm,
-    ql, qg, lg, og, table,
-    lat, wbuf, qbuf, kbuf, vbuf, latn, kturn, qfull, qnorm, gall, squares, acc, asked,
+    ql, ql_outer, qg, lg, og, table,
+    lat, wbuf, qbuf, kbuf, vbuf, latn, kturn, qfull, qfull_outer, qnorm, gall, squares, squares_outer, tally,
+    acc, asked,
     far_out, far_in, out,
     local, w_local, o_local, l_send, l_recv, g_send, g_recv,
-    w_send, w_recv, q_send, q_recv, h_send, h_recv, f_send, f_recv,
+    w_send, w_recv, m_recv, q_send, q_recv, h_send, h_recv, f_send, f_recv,
 ):
     z, t, g = lax.axis_index("sp"), lax.axis_index("tp"), lax.axis_index("grp")
     parity = lax.rem(g, 2)
@@ -171,7 +169,7 @@
     block_rows = ql.shape[0]
     depth = ow.shape[0]
     half = depth // 2
-    piece = half // SPLIT
+    piece = half // 2
     tile = wbuf.shape[3]
     heads = kup.shape[1] // NOPE_DIM
     cols = heads * VALUE_DIM
@@ -189,7 +187,9 @@
     edge = jnp.logical_or(z == 0, z == n_sp - 1)
     inner = jnp.logical_not(edge)
     far_base = jnp.where(lower, n_tp // 2, 0)
-    far_order = [*range(CHUNKS - TAIL, CHUNKS), *range(CHUNKS - TAIL)]
+    far_group = jnp.logical_and(t >= far_base, t < far_base + n_tp // 2)
+    helps = jnp.logical_and(inner, far_group)
+    helped = jnp.logical_and(edge, far_group)
 
     loads = [
         pltpu.make_async_copy(src, dst, local.at[i])
@@ -206,11 +206,19 @@
             (og_hbm, og),
         ))
     ]
-    w_loads = [
-        pltpu.make_async_copy(ow.at[:, pl.ds(f * tile, tile)], wbuf.at[z, f], w_local.at[f])
-        for f in range(TILES)
-    ]
-    for load in loads[:2] + w_loads[:1] + loads[2:5] + w_loads[1:] + loads[5:]:
+    def w_load(f):
+        return pltpu.make_async_copy(
+            ow.at[:, pl.ds(f * tile, tile)], wbuf.at[z, f], w_local.at[min(f, 1)]
+        )
+
+    for load in loads[:3]:
+        load.start()
+    w_load(0).start()
+    for load in loads[3:5]:
+        load.start()
+    for f in range(1, TILES):
+        w_load(f).start()
+    for load in loads[5:]:
         load.start()
 
     barrier = pltpu.get_barrier_semaphore()
@@ -234,14 +242,21 @@
             device_id=target, device_id_type=MESH,
         )
 
+    opposite = lax.rem(t + n_tp // 2, n_tp)
+
+    def drain(ref, send):
+        remote(ref, ref, send, send, {"tp": opposite}).wait_send()
+
+    def expect(ref, recv):
+        remote(ref, ref, recv, recv, {"tp": opposite}).wait_recv()
+
     def part_along(b, up):
-        return remote(
-            lat.at[b, t], lat.at[b, t], l_send.at[b, up], l_recv.at[b, t], {"sp": z + 1 if up else z - 1}
-        )
+        way = jnp.where(lower, 1 - up, up)
+        return remote(lat.at[b, t], lat.at[b, t], l_send.at[way], l_recv.at[b], {"sp": z + 1 if up else z - 1})
 
     def part_across(b, d):
         return remote(
-            lat.at[b, t], lat.at[b, t], l_send.at[b, 1 + d], l_recv.at[b, t], {"tp": lax.rem(t + d, n_tp)}
+            lat.at[b, t], lat.at[b, t], l_send.at[2], l_recv.at[n_sp], {"tp": lax.rem(t + d, n_tp)}
         )
 
     def spread(b):
@@ -269,99 +284,143 @@
 
             spread(z + d)
 
-    def rows_of(b, p, i):
-        start = pl.multiple_of(p * half + (i % SPLIT) * piece, piece)
-        return wbuf.at[b, i // SPLIT, pl.ds(start, piece)]
-
-    def moved(kind, b, p, i, target):
-        return remote(rows_of(b, p, i), rows_of(b, p, i), w_send.at[kind, i], w_recv.at[b, p, i], target)
-
-    def inward(i):
-        return moved(0, z, parity, i, {"sp": centre})
-
-    def outward(i):
-        return moved(1, z, parity, i, {"sp": outer})
-
-    def passed(i):
-        return moved(2, outer, parity, i, {"sp": centre})
-
-    def inward_far(i):
-        return moved(3, z, 1 - parity, i, {"sp": centre})
-
-    def passed_far(i):
-        return moved(6, outer, 1 - parity, i, {"sp": centre})
-
-    def across(b, i):
-        return moved(4, b, parity, i, {"grp": partner})
-
-    def across_beyond(i):
-        return moved(5, beyond, parity, i, {"grp": partner})
-
-    def landed(b, p, i):
-        moved(0, b, p, i, {"sp": centre}).wait_recv()
-
-    def near(i):
-        if i % SPLIT == 0:
-            w_loads[i // SPLIT].wait()
-        inward(i).start()
-
-    def near_out(i):
+    NEAR_OUTER, NEAR_CENTRE, BEYOND_NEAR, BEYOND_FAR = range(4)
+    CENTRE_FAR, TAIL_TILE, TAIL_PIECE, REST_TILES, REST_PIECE = range(5)
+    last, split = TILES - 1, TILES - 2
+
+    def rows_of(b, p, f, start=0, rows=None):
+        return wbuf.at[b, f, pl.ds(pl.multiple_of(p * half + start, piece), rows or half)]
+
+    def moved(kind, ref, recv, target):
+        return remote(ref, ref, w_send.at[kind], recv, target)
+
+    def inward(f):
+        role = jnp.where(edge, NEAR_OUTER, NEAR_CENTRE)
+        return moved(0, rows_of(z, parity, f), w_recv.at[role, f], {"sp": centre})
+
+    def outward(f):
+        return moved(1, rows_of(z, parity, f), w_recv.at[NEAR_CENTRE, f], {"sp": outer})
+
+    def passed(f):
+        return moved(2, rows_of(outer, parity, f), w_recv.at[BEYOND_NEAR, f], {"sp": centre})
+
+    def inward_far(ref, part):
+        return moved(3, ref, m_recv.at[part], {"sp": centre})
+
+    def across(f):
+        return moved(4, rows_of(centre, parity, f), m_recv.at[CENTRE_FAR], {"grp": partner})
+
+    def across_beyond(f):
+        return moved(5, rows_of(beyond, parity, f), w_recv.at[BEYOND_FAR, f], {"grp": partner})
+
+    def across_piece():
+        return moved(
+            6, rows_of(beyond, parity, split, 0, piece), w_recv.at[BEYOND_FAR, split], {"grp": partner}
+        )
+
+    def passed_far():
+        return (
+            moved(7, rows_of(outer, 1 - parity, last), w_recv.at[BEYOND_FAR, last], {"sp": centre}),
+            moved(
+                7, rows_of(outer, 1 - parity, split, piece, piece), w_recv.at[BEYOND_FAR, split], {"sp": centre}
+            ),
+        )
+
+    def landed(role, f):
+        expect(wbuf.at[0, f, pl.ds(0, half)], w_recv.at[role, f])
+
+    def near(f):
+        if f == 0:
+            w_load(0).wait()
+        if f == 1:
+            rest = wbuf.at[z, pl.ds(1, last)]
+            pltpu.make_async_copy(rest, rest, w_local.at[1]).wait()
+        inward(f).start()
+
+    def near_out(f):
         @pl.when(inner)
         def _():
-            outward(i).start()
-
-    def near_far(some):
+            outward(f).start()
+
+    def near_far():
         @pl.when(edge)
         def _():
-            for i in some:
-                inward_far(i).start()
-
-    def to_partner(i):
-        landed(centre, parity, i)
-        across(centre, i).start()
-
-    def inner_hop(some):
+            inward_far(rows_of(z, 1 - parity, last), TAIL_TILE).start()
+            inward_far(rows_of(z, 1 - parity, split, piece, piece), TAIL_PIECE).start()
+            for f in range(split):
+                inward_far(rows_of(z, 1 - parity, f), REST_TILES).start()
+            inward_far(rows_of(z, 1 - parity, split, 0, piece), REST_PIECE).start()
+
+    def to_partner(f):
+        landed(NEAR_CENTRE, f)
+        across(f).start()
+
+    def inner_partner(some):
         @pl.when(inner)
         def _():
-            for i in some:
-                landed(outer, parity, i)
-                passed(i).start()
-                to_partner(i)
-
-    def edge_hop(some):
+            for f in some:
+                to_partner(f)
+
+    def inner_pass(some):
+        @pl.when(inner)
+        def _():
+            for f in some:
+                landed(NEAR_OUTER, f)
+                passed(f).start()
+
+    def edge_partner(some):
         @pl.when(edge)
         def _():
-            for i in some:
-                to_partner(i)
-
-    def second_hop(i):
-        landed(beyond, parity, i)
-        if i < CHUNKS - TAIL:
-            across_beyond(i).start()
+            for f in some:
+                to_partner(f)
+
+    def second_hop(f):
+        landed(BEYOND_NEAR, f)
+        if f < split:
+            across_beyond(f).start()
+        if f == split:
+            across_piece().start()
 
     def first_hop_far():
-        for i in range(CHUNKS - TAIL, CHUNKS):
-            landed(outer, 1 - parity, i)
-            passed_far(i).start()
-
-    def queries():
-        for load in loads[2:5]:
-            load.wait()
-        wide = ql[...].astype(jnp.float32)
+        expect(wbuf.at[0, 0, pl.ds(0, half)], m_recv.at[TAIL_TILE])
+        expect(wbuf.at[0, 0, pl.ds(0, piece)], m_recv.at[TAIL_PIECE])
+        for copy in passed_far():
+            copy.start()
+
+    def outer_rest():
+        expect(wbuf.at[0, pl.ds(0, split), pl.ds(0, half)], m_recv.at[REST_TILES])
+        expect(wbuf.at[0, 0, pl.ds(0, piece)], m_recv.at[REST_PIECE])
+
+    def centre_far():
+        expect(wbuf.at[0, :, pl.ds(0, half)], m_recv.at[CENTRE_FAR])
+
+    def project(latent, full):
+        wide = latent[...].astype(jnp.float32)
         mean = jnp.mean(wide * wide, axis=-1, keepdims=True)
         gain = jnp.concatenate([qg[i : i + 1] for i in range(qg.shape[0])], axis=1)
         qnorm[...] = (wide * lax.rsqrt(mean + norm_eps) * gain).astype(jnp.bfloat16)
-        qfull[...] = jnp.dot(qnorm[...], qbuf[...], preferred_element_type=jnp.float32).astype(
+        full[...] = jnp.dot(qnorm[...], qbuf[...], preferred_element_type=jnp.float32).astype(
             jnp.bfloat16
         )
+
+    def lend():
+        return remote(ql, ql_outer, h_send.at[1], h_recv.at[1], {"sp": centre})
+
+    def queries():
+        for load in loads[3:5]:
+            load.wait()
+        project(ql, qfull)
+
+    def outer_queries():
+        @pl.when(helps)
+        def _():
+            lend().wait_recv()
+            project(ql_outer, qfull_outer)
 
     def latents():
         for load in loads[5:]:
             load.wait()
-        for b in range(n_sp):
-            for d in range(1, n_tp):
-                p = lax.rem(t + d, n_tp)
-                remote(lat.at[b, p], lat.at[b, p], l_send.at[b, 1 + d], l_recv.at[b, p], {"tp": p}).wait_recv()
+        expect(lat.at[:, pl.ds(0, n_tp - 1)], l_recv.at[n_sp])
         whole = lat[...].reshape(keys, rank + width)
         wide = whole[:, :rank].astype(jnp.float32)
         mean = jnp.mean(wide * wide, axis=-1, keepdims=True)
@@ -371,11 +430,11 @@
 
     transposed = (((1,), (1,)), ((), ()))
 
-    def attend(h):
+    def attend_with(h, full, block, store, squares):
         start = h * head_width
-        plain = qfull[:, start : start + NOPE_DIM]
-        spun = qfull[:, start + NOPE_DIM : start + head_width].astype(jnp.float32)
-        own = table[pl.ds(pl.multiple_of(z * block_rows, block_rows), block_rows), :]
+        plain = full[:, start : start + NOPE_DIM]
+        spun = full[:, start + NOPE_DIM : start + head_width].astype(jnp.float32)
+        own = table[pl.ds(pl.multiple_of(block * block_rows, block_rows), block_rows), :]
         spun = turned(spun, own).astype(jnp.bfloat16)
         key_plain = jnp.dot(
             latn[...], kbuf[:, h * NOPE_DIM : (h + 1) * NOPE_DIM], preferred_element_type=jnp.float32
@@ -394,72 +453,78 @@
         ).astype(jnp.bfloat16)
         wide = head_out.astype(jnp.float32)
         gained = wide * og[:, h * VALUE_DIM : (h + 1) * VALUE_DIM]
-        gall[t, :, h * VALUE_DIM : (h + 1) * VALUE_DIM] = gained.astype(jnp.bfloat16)
+        store(gained.astype(jnp.bfloat16))
         square = jnp.sum(wide * wide, axis=-1, keepdims=True)
         if h:
             square = square + squares[:, :1]
         squares[...] = jnp.broadcast_to(square, squares.shape)
+
+    def attend(h):
+        def store(value):
+            gall[t, :, h * VALUE_DIM : (h + 1) * VALUE_DIM] = value
+
+        attend_with(h, qfull, z, store, squares)
         if h == heads - 1:
             gall[t, :, cols:] = squares[...].astype(jnp.bfloat16)
 
+    def attend_outer(h):
+        def store(value):
+            asked[core, :, h * VALUE_DIM : (h + 1) * VALUE_DIM] = value
+
+        attend_with(h, qfull_outer, outer, store, squares_outer)
+        if h == heads - 1:
+            tally[...] = squares_outer[...].astype(jnp.bfloat16)
+
     def is_near(p):
         return jnp.logical_or(p < far_base, p >= far_base + n_tp // 2)
 
-    def share_copy(h, d):
-        part = gall.at[t, :, pl.ds(h * VALUE_DIM, VALUE_DIM)]
-        return remote(part, part, g_send.at[h, d], g_recv.at[h, d], {"tp": lax.rem(t + d, n_tp)})
-
-    def each_share(h, d, p, act):
-        @pl.when(jnp.logical_or(inner, is_near(p)) if h < heads else True)
-        def _():
-            act(share_copy(h, d))
-
     def share(h):
-        for d in range(1, n_tp):
-            each_share(h, d, t, lambda copy: copy.start())
-        if h < heads:
-            @pl.when(asks)
+        @pl.when(jnp.logical_or(inner, is_near(t)) if h < heads else True)
+        def _():
+            for d in range(1, n_tp):
+                part = gall.at[t, :, pl.ds(h * VALUE_DIM, VALUE_DIM)]
+                kind = h // heads
+                remote(part, part, g_send.at[kind], g_recv.at[kind], {"tp": lax.rem(t + d, n_tp)}).start()
+
+    def slabs(count, span):
+        return gall.at[pl.ds(0, count), :, pl.ds(0, span)]
+
+    def gather():
+        for where, count in (
+            (inner, n_tp - 1),
+            (jnp.logical_and(edge, is_near(t)), n_tp // 2 - 1),
+            (helped, n_tp // 2),
+        ):
+            @pl.when(where)
             def _():
-                for kind in range(2):
-                    ask(h, kind).start()
-
-    def sent(h):
-        for d in range(1, n_tp):
-            each_share(h, d, t, lambda copy: copy.wait_send())
-
-    def gather(h):
-        for d in range(1, n_tp):
-            each_share(h, d, lax.rem(t + n_tp - d, n_tp), lambda copy: copy.wait_recv())
-
-    asks = jnp.logical_and(edge, jnp.logical_not(is_near(t)))
-    opposite = lax.rem(t + n_tp // 2, n_tp)
-
-    def head_of(h):
-        return pl.ds(h * VALUE_DIM, VALUE_DIM)
-
-    def ask(h, kind):
+                expect(slabs(count, cols), g_recv.at[0])
+
+        expect(slabs(n_tp - 1, VALUE_DIM), g_recv.at[1])
+
+    def ask(h):
+        part = asked.at[core, :, pl.ds(h * VALUE_DIM, VALUE_DIM)]
+        return remote(part, part, q_send.at[0], q_recv.at[0], {"tp": opposite})
+
+    def tell():
         return remote(
-            gall.at[t, :, head_of(h)], asked.at[core, :, head_of(h)],
-            q_send.at[kind, h], q_recv.at[h], {"sp": centre, "tp": opposite} if kind else {"sp": centre},
-        )
-
-    def pair_of(a):
-        return pl.ds(a * (cols // 2), cols // 2)
-
-    def hand(c, a):
-        part = asked.at[c, :, pair_of(a)]
-        return remote(part, part, h_send.at[a], h_recv.at[a], {"tp": sibling})
-
-    def hand_on(a):
-        for h in range(a * heads // 2, (a + 1) * heads // 2):
-            ask(h, 0).wait_recv()
-        hand(core, a).start()
-
-    def heard(a):
-        hand(1 - core, a).wait_recv()
+            tally, gall.at[t, :, pl.ds(cols, VALUE_DIM)], h_send.at[2], h_recv.at[2], {"sp": outer}
+        )
+
+    def hand(c):
+        return remote(asked.at[c], asked.at[c], h_send.at[0], h_recv.at[0], {"tp": sibling})
+
+    def hand_on():
+        @pl.when(jnp.logical_not(helps))
+        def _():
+            expect(asked.at[0], q_recv.at[0])
+
+        hand(core).start()
+
+    def heard():
+        hand(1 - core).wait_recv()
 
     def answer(f):
-        return remote(far_out.at[f], far_in.at[f], f_send.at[f], f_recv.at[f], {"sp": outer})
+        return remote(far_out.at[f], far_in.at[f], f_send.at[0], f_recv.at[f], {"sp": outer})
 
     def part_of(p):
         return pl.ds(pl.multiple_of(p * half, half), half)
@@ -479,7 +544,7 @@
             acc[f] = part if fresh else acc[f] + part
 
     def stored(f):
-        return pltpu.make_async_copy(out.at[f], out_hbm.at[:, pl.ds(f * tile, tile)], o_local.at[f])
+        return pltpu.make_async_copy(out.at[f], out_hbm.at[:, pl.ds(f * tile, tile)], o_local.at[0])
 
     def set_scale():
         square = gall[0, :, cols : cols + 1].astype(jnp.float32)
@@ -498,9 +563,6 @@
     tiles = range(TILES)
     pairs = [(f, f + 1) for f in range(0, TILES, 2)]
 
-    def chunks_of(some):
-        return range(some[0] * SPLIT, (some[-1] + 1) * SPLIT)
-
     loads[0].wait()
     loads[1].wait()
 
@@ -513,147 +575,177 @@
         part_along(z, 0).start()
 
     spread(z)
-    run(near, range(5))
+    loads[2].wait()
+
+    @pl.when(helped)
+    def _():
+        lend().start()
+
+    run(near, range(2))
     queries()
     arrive(1)
-    run(near, range(5, CHUNKS))
-    run(near_out, range(4))
+    run(near, range(2, TILES))
+    run(near_out, range(2))
+    inner_partner(range(2))
     arrive(2)
-    run(near_out, range(4, CHUNKS))
-    inner_hop(range(4))
+    run(near_out, range(2, TILES))
+    inner_partner(range(2, 3))
     arrive(3)
-    inner_hop(range(4, 6))
-    near_far(far_order[:4])
+    near_far()
+    outer_queries()
+    inner_partner(range(3, 4))
     latents()
-    inner_hop(range(6, 8))
-    attend(0)
-    inner_hop(range(8, 10))
-    edge_hop(range(6))
-    near_far(far_order[4:8])
-    attend(1)
-    share(0)
-    inner_hop(range(10, 12))
-    edge_hop(range(6, 8))
-    attend(2)
-    share(1)
-    inner_hop(range(12, 14))
-    edge_hop(range(8, 9))
-    near_far(far_order[8:12])
-    attend(3)
-    share(2)
-    inner_hop(range(14, CHUNKS))
-    edge_hop(range(9, 11))
-
-    @pl.when(inner)
-    def _():
-        first_hop_far()
-        run(second_hop, range(2))
-
-    share(3)
+    inner_partner(range(4, 5))
+    inner_pass(range(2))
+
+    @pl.when(helps)
+    def _():
+        attend_outer(0)
+        run(to_partner, range(5, 6))
+        attend_outer(1)
+        ask(0).start()
+        inner_pass(range(2, 4))
+        run(to_partner, range(6, 7))
+        attend_outer(2)
+        ask(1).start()
+        inner_pass(range(4, 5))
+        attend_outer(3)
+        ask(2).start()
+        run(to_partner, range(7, TILES))
+        inner_pass(range(5, 6))
+        ask(3).start()
+        tell().start()
+        attend(0)
+        hand_on()
+        inner_pass(range(6, 7))
+        attend(1)
+        share(0)
+        run(second_hop, range(1))
+        attend(2)
+        share(1)
+        inner_pass(range(7, TILES))
+        run(second_hop, range(1, 2))
+        attend(3)
+        share(2)
+        run(second_hop, range(2, 3))
+        share(3)
+
+    @pl.when(is_near(t))
+    def _():
+        attend(0)
+        inner_partner(range(5, 6))
+        inner_pass(range(2, 4))
+        edge_partner(range(5))
+        attend(1)
+        share(0)
+        inner_pass(range(4, 5))
+        edge_partner(range(5, 6))
+        attend(2)
+        share(1)
+        inner_partner(range(6, 7))
+        inner_pass(range(5, 6))
+        edge_partner(range(6, 7))
+        attend(3)
+        share(2)
+        inner_partner(range(7, TILES))
+        inner_pass(range(6, TILES))
+        edge_partner(range(7, TILES))
+        share(3)
+
+        @pl.when(inner)
+        def _():
+            run(second_hop, range(2))
+            hand_on()
+            run(second_hop, range(2, 3))
+
+    @pl.when(helped)
+    def _():
+        run(to_partner, tiles)
+        tell().wait_recv()
+
     share(heads)
 
     @pl.when(edge)
     def _():
-        run(to_partner, range(11, 13))
-        for i in far_order[12:]:
-            inward_far(i).start()
-        run(to_partner, range(13, CHUNKS))
-        for h in range(heads + 1):
-            gather(h)
+        gather()
         set_scale()
         for some in pairs:
             keep(some, dot(gained(z), z, some), fresh=True)
+        centre_far()
         for some in pairs:
-            for i in chunks_of(some):
-                landed(centre, 1 - parity, i)
             keep(some, dot(gained(centre), centre, some))
         for f in tiles:
             answer(f).wait_recv()
             put(f, acc[f] + far_in[f].astype(jnp.float32))
 
+    def reply(f):
+        landed(BEYOND_FAR, f)
+        far = dot(asked[beyond - far_base], beyond, (f,)) + dot(asked[centre - far_base], centre, (f,))
+        far_out[f] = far.astype(far_out.dtype)
+        answer(f).start()
+
     @pl.when(inner)
     def _():
-        run(second_hop, range(2, 7))
-        for h in range(heads + 1):
-            gather(h)
-        run(second_hop, range(7, 8))
+        first_hop_far()
+        run(second_hop, range(3, 4))
+        heard()
+        centre_far()
+        for f in range(4):
+            reply(f)
+            run(second_hop, range(f + 4, f + 5))
+        reply(4)
+        gather()
         set_scale()
+        for some in pairs[:2]:
+            keep(some, dot(gained(z), z, some) + dot(gained(centre), centre, some), fresh=True)
+        reply(5)
+        for some in pairs[2:]:
+            keep(some, dot(gained(z), z, some) + dot(gained(centre), centre, some), fresh=True)
+        reply(6)
+        reply(7)
+        outer_rest()
         for some in pairs:
-            keep(some, dot(gained(z), z, some), fresh=True)
-        hand_on(0)
-        run(second_hop, range(8, 9))
-        for i in range(CHUNKS):
-            landed(centre, 1 - parity, i)
-        for some in pairs:
-            keep(some, dot(gained(centre), centre, some))
-        hand_on(1)
-        run(second_hop, range(9, 11))
-        for a in range(2):
-            heard(a)
-        for some in pairs[:-1] + [(f,) for f in pairs[-1]]:
-            run(second_hop, [i for i in chunks_of(some) if i >= 11])
-            for i in chunks_of(some):
-                landed(beyond, 1 - parity, i)
-            both = jnp.concatenate([gained(beyond), asked[beyond - far_base]], axis=0)
-            both = dot(both, beyond, some)
-            far = both[block_rows:] + dot(asked[centre - far_base], centre, some)
-            for n, f in enumerate(some):
-                far_out[f] = far[:, n * tile : (n + 1) * tile].astype(far_out.dtype)
-            for f in some:
-                answer(f).start()
-            keep(some, both[:block_rows])
-        for i in range(CHUNKS - TAIL):
-            landed(outer, 1 - parity, i)
-        for some in pairs:
-            total = dot(gained(outer), outer, some)
+            total = dot(gained(outer), outer, some) + dot(gained(beyond), beyond, some)
             for n, f in enumerate(some):
                 put(f, acc[f] + total[:, n * tile : (n + 1) * tile])
 
-    for b in range(n_sp):
-        for d in range(1, n_tp):
-            part_across(b, d).wait_send()
-
-        @pl.when(jnp.logical_and(z >= b, has_up))
-        def _():
-            part_along(b, 1).wait_send()
-
-        @pl.when(jnp.logical_and(z <= b, has_down))
-        def _():
-            part_along(b, 0).wait_send()
-
-    for h in range(heads + 1):
-        sent(h)
-    for i in range(CHUNKS):
-        inward(i).wait_send()
-        across(centre, i).wait_send()
+    halves = wbuf.at[0, :, pl.ds(0, half)]
+    drain(lat.at[:, pl.ds(0, n_tp - 1)], l_send.at[2])
+    drain(slabs(n_tp - 1, VALUE_DIM), g_send.at[1])
+    drain(halves, w_send.at[0])
+    drain(halves, w_send.at[4])
+
+    @pl.when(jnp.logical_or(inner, is_near(t)))
+    def _():
+        drain(slabs(n_tp - 1, cols), g_send.at[0])
 
     @pl.when(edge)
     def _():
-        for i in range(CHUNKS):
-            inward_far(i).wait_send()
-
-    @pl.when(asks)
-    def _():
-        for h in range(heads):
-            for kind in range(2):
-                ask(h, kind).wait_send()
+        drain(lat.at[0, pl.ds(0, 1)], l_send.at[0])
+        drain(halves, w_send.at[3])
+
+    @pl.when(helped)
+    def _():
+        lend().wait_send()
+
+    @pl.when(helps)
+    def _():
+        drain(asked.at[0], q_send.at[0])
+        tell().wait_send()
 
     @pl.when(inner)
     def _():
-        for i in range(CHUNKS):
-            outward(i).wait_send()
-            passed(i).wait_send()
-            if i < CHUNKS - TAIL:
-                across_beyond(i).wait_send()
-            else:
-                passed_far(i).wait_send()
-        for a in range(2):
-            hand(core, a).wait_send()
-        for f in range(TILES):
-            answer(f).wait_send()
-
-    for f in range(TILES):
-        stored(f).wait()
+        drain(lat.at[0, pl.ds(0, 2)], l_send.at[0])
+        drain(lat.at[0, pl.ds(0, 3)], l_send.at[1])
+        drain(halves, w_send.at[1])
+        drain(halves, w_send.at[2])
+        drain(wbuf.at[0, pl.ds(0, split), pl.ds(0, half)], w_send.at[5])
+        across_piece().wait_send()
+        drain(wbuf.at[0, 0, pl.ds(0, half + piece)], w_send.at[7])
+        hand(core).wait_send()
+        drain(far_out, f_send.at[0])
+
+    pltpu.make_async_copy(out, out, o_local.at[0]).wait()
 
 
 MESH = pl.DeviceIdType.MESH
@@ -680,6 +772,7 @@
         out_specs=in_hbm,
         scratch_shapes=[
             vmem(query_latent.shape, bf16),
+            vmem(query_latent.shape, bf16),
             vmem((query_gain.shape[0] // LANES, LANES), jnp.float32),
             vmem((1, rank), jnp.float32),
             vmem((1, cols), jnp.float32),
@@ -692,28 +785,32 @@
             vmem((keys, rank), bf16),
             vmem((keys, width), bf16),
             vmem((block_rows, query_up.shape[1]), bf16),
+            vmem((block_rows, query_up.shape[1]), bf16),
             vmem(query_latent.shape, bf16),
             vmem((n_tp, block_rows, cols + VALUE_DIM), bf16),
             vmem((block_rows, VALUE_DIM), jnp.float32),
+            vmem((block_rows, VALUE_DIM), jnp.float32),
+            vmem((block_rows, VALUE_DIM), bf16),
             vmem(tiled, jnp.float32),
             vmem((n_tp // 2, block_rows, cols), bf16),
             vmem(tiled, bf16),
             vmem(tiled, bf16),
             vmem(tiled, bf16),
             dma((10,)),
-            dma((TILES,)),
-            dma((TILES,)),
-            dma((n_sp, n_tp + 1)),
-            dma((n_sp, n_tp)),
-            dma((cols // VALUE_DIM + 1, n_tp)),
-            dma((cols // VALUE_DIM + 1, n_tp)),
-            dma((7, CHUNKS)),
-            dma((n_sp, 2, CHUNKS)),
-            dma((2, cols // VALUE_DIM)),
-            dma((cols // VALUE_DIM,)),
+            dma((2,)),
+            dma((1,)),
+            dma((3,)),
+            dma((n_sp + 1,)),
             dma((2,)),
             dma((2,)),
-            dma((TILES,)),
+            dma((8,)),
+            dma((4, TILES)),
+            dma((5,)),
+            dma((1,)),
+            dma((1,)),
+            dma((3,)),
+            dma((3,)),
+            dma((1,)),
             dma((TILES,)),
         ],
         compiler_params=pltpu.CompilerParams(

time: 49.2 us -> 39.3 us (0.80)
  Pallas kernels: 47.4 us -> 37.4 us
    pallas_call x1, Pallas kernels: 47.4 us -> 37.4 us  [on_device_fused(): pl.pallas_call(functools.partial(kernel, n_sp, n_tp), out_shape=jax.Shape...]
where the time goes in v3:
time: 39.3 us; the launch traced here: 39.1 us
  Pallas kernels  37.4 us (95%)
  local copies, waits for them, and re-layouts  1.67 us (4%)
    pallas_call x1, Pallas kernels, on_device_fused(): pl.pallas_call(functools.partial(kernel, n_sp, n_tp), out_shape=jax.Shape...  37.4 us
    unnamed x1, local copies, waits for them, and re-layouts  1.67 us

profile of v3, /device:TPU:0, one launch (start us, length us, event | category | flops | bytes accessed | tf_op | source)
XLA Modules:
  0.0 39.1 jit_solution(12120548948824885737)
XLA Ops:
  0.0 37.4 %shard_map.109 = bf16[128,1024]{1,0:T(8,128)(2,1)} custom-call(bf16[128,768]{1,0:T(8,128)(2,1)} %ql_hbm.1, bf16[32,256]{1,0:T(8,128)(2,1)} %kl.1, bf16[32,64]{1,0:T(8,128)(2,1)} %rk.1, f32[6,128]{1,0:T(8,128)} %bitcast.3, f32[1,256]{1,0:T(1,128)} %bitcast.5, f32[1,512]{1,0:T(1,128)} %bitcast.4, f32[512,128]{1,0:T(8,128)} %constant.2.clone.table_hbm, ...), custom_call_target="tpu_custom_call" | custom-call | tf_op jit(solution)/shard_map/pallas_call | solution.py:768
  37.4 1.7 %copy.13 = bf16[128,1024]{1,0:T(8,128)(2,1)} copy(bf16[128,1024]{1,0:T(8,128)(2,1)} %shard_map.109) | data formatting | bytes 524288

commit v4 on v3

--- a/solution.py
+++ b/solution.py
@@ -158,8 +158,7 @@
     lat, wbuf, qbuf, kbuf, vbuf, latn, kturn, qfull, qfull_outer, qnorm, gall, squares, squares_outer, tally,
     acc, asked,
     far_out, far_in, out,
-    local, w_local, o_local, l_send, l_recv, g_send, g_recv,
-    w_send, w_recv, m_recv, q_send, q_recv, h_send, h_recv, f_send, f_recv,
+    local, w_local, o_local, sends, l_recv, g_recv, w_recv, m_recv, q_recv, h_recv, f_recv,
 ):
     z, t, g = lax.axis_index("sp"), lax.axis_index("tp"), lax.axis_index("grp")
     parity = lax.rem(g, 2)
@@ -193,18 +192,18 @@
 
     loads = [
         pltpu.make_async_copy(src, dst, local.at[i])
-        for i, (src, dst) in enumerate((
-            (kl, lat.at[z, t, :, pl.ds(0, rank)]),
-            (rk, lat.at[z, t, :, pl.ds(rank, width)]),
-            (ql_hbm, ql),
-            (qg_hbm, qg),
-            (qup, qbuf),
-            (lg_hbm, lg),
-            (table_hbm, table),
-            (kup, kbuf),
-            (vup, vbuf),
-            (og_hbm, og),
-        ))
+        for i, src, dst in (
+            (0, kl, lat.at[z, t, :, pl.ds(0, rank)]),
+            (0, rk, lat.at[z, t, :, pl.ds(rank, width)]),
+            (1, ql_hbm, ql),
+            (2, qg_hbm, qg),
+            (2, qup, qbuf),
+            (3, lg_hbm, lg),
+            (3, table_hbm, table),
+            (3, kup, kbuf),
+            (3, vup, vbuf),
+            (3, og_hbm, og),
+        )
     ]
     def w_load(f):
         return pltpu.make_async_copy(
@@ -236,28 +235,25 @@
         pl.semaphore_signal(barrier, inc=1, device_id={"tp": lax.rem(t + d, n_tp)}, device_id_type=MESH)
     pl.semaphore_wait(barrier, n_tp + jnp.where(edge, 1, 2))
 
-    def remote(src, dst, send, recv, target):
+    def remote(src, dst, recv, target):
         return pltpu.make_async_remote_copy(
-            src_ref=src, dst_ref=dst, send_sem=send, recv_sem=recv,
+            src_ref=src, dst_ref=dst, send_sem=sends.at[0], recv_sem=recv,
             device_id=target, device_id_type=MESH,
         )
 
     opposite = lax.rem(t + n_tp // 2, n_tp)
 
-    def drain(ref, send):
-        remote(ref, ref, send, send, {"tp": opposite}).wait_send()
+    def drain(ref):
+        remote(ref, ref, sends.at[0], {"tp": opposite}).wait_send()
 
     def expect(ref, recv):
-        remote(ref, ref, recv, recv, {"tp": opposite}).wait_recv()
+        remote(ref, ref, recv, {"tp": opposite}).wait_recv()
 
     def part_along(b, up):
-        way = jnp.where(lower, 1 - up, up)
-        return remote(lat.at[b, t], lat.at[b, t], l_send.at[way], l_recv.at[b], {"sp": z + 1 if up else z - 1})
+        return remote(lat.at[b, t], lat.at[b, t], l_recv.at[b], {"sp": z + 1 if up else z - 1})
 
     def part_across(b, d):
-        return remote(
-            lat.at[b, t], lat.at[b, t], l_send.at[2], l_recv.at[n_sp], {"tp": lax.rem(t + d, n_tp)}
-        )
+        return remote(lat.at[b, t], lat.at[b, t], l_recv.at[n_sp], {"tp": lax.rem(t + d, n_tp)})
 
     def spread(b):
         for d in range(1, n_tp):
@@ -284,50 +280,48 @@
 
             spread(z + d)
 
-    NEAR_OUTER, NEAR_CENTRE, BEYOND_NEAR, BEYOND_FAR = range(4)
+    FROM_OUTER = 0
+    FROM_CENTRE, BEYOND_NEAR, BEYOND_FAR = (TILES // 2 + TILES * i for i in range(3))
     CENTRE_FAR, TAIL_TILE, TAIL_PIECE, REST_TILES, REST_PIECE = range(5)
     last, split = TILES - 1, TILES - 2
 
     def rows_of(b, p, f, start=0, rows=None):
         return wbuf.at[b, f, pl.ds(pl.multiple_of(p * half + start, piece), rows or half)]
 
-    def moved(kind, ref, recv, target):
-        return remote(ref, ref, w_send.at[kind], recv, target)
+    def moved(ref, recv, target):
+        return remote(ref, ref, recv, target)
 
     def inward(f):
-        role = jnp.where(edge, NEAR_OUTER, NEAR_CENTRE)
-        return moved(0, rows_of(z, parity, f), w_recv.at[role, f], {"sp": centre})
+        role = jnp.where(edge, FROM_OUTER + f // 2, FROM_CENTRE + f)
+        return moved(rows_of(z, parity, f), w_recv.at[role], {"sp": centre})
 
     def outward(f):
-        return moved(1, rows_of(z, parity, f), w_recv.at[NEAR_CENTRE, f], {"sp": outer})
+        return moved(rows_of(z, parity, f), w_recv.at[FROM_CENTRE + f], {"sp": outer})
 
     def passed(f):
-        return moved(2, rows_of(outer, parity, f), w_recv.at[BEYOND_NEAR, f], {"sp": centre})
+        return moved(rows_of(outer, parity, f), w_recv.at[BEYOND_NEAR + f], {"sp": centre})
 
     def inward_far(ref, part):
-        return moved(3, ref, m_recv.at[part], {"sp": centre})
+        return moved(ref, m_recv.at[part], {"sp": centre})
 
     def across(f):
-        return moved(4, rows_of(centre, parity, f), m_recv.at[CENTRE_FAR], {"grp": partner})
+        return moved(rows_of(centre, parity, f), m_recv.at[CENTRE_FAR], {"grp": partner})
 
     def across_beyond(f):
-        return moved(5, rows_of(beyond, parity, f), w_recv.at[BEYOND_FAR, f], {"grp": partner})
+        return moved(rows_of(beyond, parity, f), w_recv.at[BEYOND_FAR + f], {"grp": partner})
 
     def across_piece():
         return moved(
-            6, rows_of(beyond, parity, split, 0, piece), w_recv.at[BEYOND_FAR, split], {"grp": partner}
-        )
-
-    def passed_far():
-        return (
-            moved(7, rows_of(outer, 1 - parity, last), w_recv.at[BEYOND_FAR, last], {"sp": centre}),
-            moved(
-                7, rows_of(outer, 1 - parity, split, piece, piece), w_recv.at[BEYOND_FAR, split], {"sp": centre}
-            ),
+            rows_of(beyond, parity, split, 0, piece), w_recv.at[BEYOND_FAR + split], {"grp": partner}
+        )
+
+    def pass_tail(f, start=0, rows=None):
+        return moved(
+            rows_of(outer, 1 - parity, f, start, rows), w_recv.at[BEYOND_FAR + f], {"sp": centre}
         )
 
     def landed(role, f):
-        expect(wbuf.at[0, f, pl.ds(0, half)], w_recv.at[role, f])
+        expect(wbuf.at[0, f, pl.ds(0, half)], w_recv.at[role + f])
 
     def near(f):
         if f == 0:
@@ -345,14 +339,14 @@
     def near_far():
         @pl.when(edge)
         def _():
+            inward_far(rows_of(z, 1 - parity, split, piece, piece), TAIL_PIECE).start()
+            inward_far(rows_of(z, 1 - parity, split, 0, piece), REST_PIECE).start()
             inward_far(rows_of(z, 1 - parity, last), TAIL_TILE).start()
-            inward_far(rows_of(z, 1 - parity, split, piece, piece), TAIL_PIECE).start()
             for f in range(split):
                 inward_far(rows_of(z, 1 - parity, f), REST_TILES).start()
-            inward_far(rows_of(z, 1 - parity, split, 0, piece), REST_PIECE).start()
 
     def to_partner(f):
-        landed(NEAR_CENTRE, f)
+        landed(FROM_CENTRE, f)
         across(f).start()
 
     def inner_partner(some):
@@ -361,11 +355,11 @@
             for f in some:
                 to_partner(f)
 
-    def inner_pass(some):
+    def inner_pass(pair):
         @pl.when(inner)
         def _():
-            for f in some:
-                landed(NEAR_OUTER, f)
+            expect(wbuf.at[0, pl.ds(0, 2), pl.ds(0, half)], w_recv.at[FROM_OUTER + pair])
+            for f in (2 * pair, 2 * pair + 1):
                 passed(f).start()
 
     def edge_partner(some):
@@ -379,17 +373,28 @@
         if f < split:
             across_beyond(f).start()
         if f == split:
-            across_piece().start()
-
-    def first_hop_far():
+            @pl.when(core == 1)
+            def _():
+                across_piece().start()
+
+    def pass_tails():
+        expect(wbuf.at[0, 0, pl.ds(0, piece)], m_recv.at[TAIL_PIECE])
+        pass_tail(split, piece, piece).start()
+
+        @pl.when(core == 0)
+        def _():
+            expect(wbuf.at[0, 0, pl.ds(0, piece)], m_recv.at[REST_PIECE])
+            pass_tail(split, 0, piece).start()
+
         expect(wbuf.at[0, 0, pl.ds(0, half)], m_recv.at[TAIL_TILE])
-        expect(wbuf.at[0, 0, pl.ds(0, piece)], m_recv.at[TAIL_PIECE])
-        for copy in passed_far():
-            copy.start()
+        pass_tail(last).start()
 
     def outer_rest():
         expect(wbuf.at[0, pl.ds(0, split), pl.ds(0, half)], m_recv.at[REST_TILES])
-        expect(wbuf.at[0, 0, pl.ds(0, piece)], m_recv.at[REST_PIECE])
+
+        @pl.when(core == 1)
+        def _():
+            expect(wbuf.at[0, 0, pl.ds(0, piece)], m_recv.at[REST_PIECE])
 
     def centre_far():
         expect(wbuf.at[0, :, pl.ds(0, half)], m_recv.at[CENTRE_FAR])
@@ -404,7 +409,7 @@
         )
 
     def lend():
-        return remote(ql, ql_outer, h_send.at[1], h_recv.at[1], {"sp": centre})
+        return remote(ql, ql_outer, h_recv.at[1], {"sp": centre})
 
     def queries():
         for load in loads[3:5]:
@@ -484,7 +489,7 @@
             for d in range(1, n_tp):
                 part = gall.at[t, :, pl.ds(h * VALUE_DIM, VALUE_DIM)]
                 kind = h // heads
-                remote(part, part, g_send.at[kind], g_recv.at[kind], {"tp": lax.rem(t + d, n_tp)}).start()
+                remote(part, part, g_recv.at[kind], {"tp": lax.rem(t + d, n_tp)}).start()
 
     def slabs(count, span):
         return gall.at[pl.ds(0, count), :, pl.ds(0, span)]
@@ -503,15 +508,13 @@
 
     def ask(h):
         part = asked.at[core, :, pl.ds(h * VALUE_DIM, VALUE_DIM)]
-        return remote(part, part, q_send.at[0], q_recv.at[0], {"tp": opposite})
+        return remote(part, part, q_recv.at[0], {"tp": opposite})
 
     def tell():
-        return remote(
-            tally, gall.at[t, :, pl.ds(cols, VALUE_DIM)], h_send.at[2], h_recv.at[2], {"sp": outer}
-        )
+        return remote(tally, gall.at[t, :, pl.ds(cols, VALUE_DIM)], h_recv.at[2], {"sp": outer})
 
     def hand(c):
-        return remote(asked.at[c], asked.at[c], h_send.at[0], h_recv.at[0], {"tp": sibling})
+        return remote(asked.at[c], asked.at[c], h_recv.at[0], {"tp": sibling})
 
     def hand_on():
         @pl.when(jnp.logical_not(helps))
@@ -523,11 +526,11 @@
     def heard():
         hand(1 - core).wait_recv()
 
+    groups = (tuple(range(split - 2)), (split - 2, split - 1), (split,), (last,))
+
     def answer(f):
-        return remote(far_out.at[f], far_in.at[f], f_send.at[0], f_recv.at[f], {"sp": outer})
-
-    def part_of(p):
-        return pl.ds(pl.multiple_of(p * half, half), half)
+        n = [f in some for some in groups].index(True)
+        return remote(far_out.at[f], far_in.at[f], f_recv.at[n], {"sp": outer})
 
     def wide_of(b, some):
         return jnp.concatenate([wbuf[b, f] for f in some], axis=1)
@@ -581,10 +584,10 @@
     def _():
         lend().start()
 
-    run(near, range(2))
+    run(near, range(3))
     queries()
     arrive(1)
-    run(near, range(2, TILES))
+    run(near, range(3, TILES))
     run(near_out, range(2))
     inner_partner(range(2))
     arrive(2)
@@ -596,7 +599,7 @@
     inner_partner(range(3, 4))
     latents()
     inner_partner(range(4, 5))
-    inner_pass(range(2))
+    inner_pass(0)
 
     @pl.when(helps)
     def _():
@@ -604,26 +607,24 @@
         run(to_partner, range(5, 6))
         attend_outer(1)
         ask(0).start()
-        inner_pass(range(2, 4))
+        inner_pass(1)
         run(to_partner, range(6, 7))
         attend_outer(2)
         ask(1).start()
-        inner_pass(range(4, 5))
+        run(to_partner, range(7, TILES))
         attend_outer(3)
         ask(2).start()
-        run(to_partner, range(7, TILES))
-        inner_pass(range(5, 6))
+        inner_pass(2)
         ask(3).start()
         tell().start()
         attend(0)
         hand_on()
-        inner_pass(range(6, 7))
+        run(second_hop, range(1))
         attend(1)
         share(0)
-        run(second_hop, range(1))
         attend(2)
         share(1)
-        inner_pass(range(7, TILES))
+        inner_pass(3)
         run(second_hop, range(1, 2))
         attend(3)
         share(2)
@@ -634,21 +635,19 @@
     def _():
         attend(0)
         inner_partner(range(5, 6))
-        inner_pass(range(2, 4))
+        inner_pass(1)
         edge_partner(range(5))
         attend(1)
         share(0)
-        inner_pass(range(4, 5))
         edge_partner(range(5, 6))
         attend(2)
         share(1)
-        inner_partner(range(6, 7))
-        inner_pass(range(5, 6))
+        inner_partner(range(6, TILES))
+        inner_pass(2)
         edge_partner(range(6, 7))
         attend(3)
         share(2)
-        inner_partner(range(7, TILES))
-        inner_pass(range(6, TILES))
+        inner_pass(3)
         edge_partner(range(7, TILES))
         share(3)
 
@@ -674,9 +673,10 @@
         centre_far()
         for some in pairs:
             keep(some, dot(gained(centre), centre, some))
-        for f in tiles:
-            answer(f).wait_recv()
-            put(f, acc[f] + far_in[f].astype(jnp.float32))
+        for n, some in enumerate(groups):
+            expect(far_in.at[pl.ds(0, len(some))], f_recv.at[n])
+            for f in some:
+                put(f, acc[f] + far_in[f].astype(jnp.float32))
 
     def reply(f):
         landed(BEYOND_FAR, f)
@@ -686,12 +686,14 @@
 
     @pl.when(inner)
     def _():
-        first_hop_far()
+        pl.when(core == 0)(pass_tails)
         run(second_hop, range(3, 4))
         heard()
         centre_far()
         for f in range(4):
             reply(f)
+            if f == 2:
+                pl.when(core == 1)(pass_tails)
             run(second_hop, range(f + 4, f + 5))
         reply(4)
         gather()
@@ -699,10 +701,10 @@
         for some in pairs[:2]:
             keep(some, dot(gained(z), z, some) + dot(gained(centre), centre, some), fresh=True)
         reply(5)
+        reply(6)
+        reply(7)
         for some in pairs[2:]:
             keep(some, dot(gained(z), z, some) + dot(gained(centre), centre, some), fresh=True)
-        reply(6)
-        reply(7)
         outer_rest()
         for some in pairs:
             total = dot(gained(outer), outer, some) + dot(gained(beyond), beyond, some)
@@ -710,40 +712,37 @@
                 put(f, acc[f] + total[:, n * tile : (n + 1) * tile])
 
     halves = wbuf.at[0, :, pl.ds(0, half)]
-    drain(lat.at[:, pl.ds(0, n_tp - 1)], l_send.at[2])
-    drain(slabs(n_tp - 1, VALUE_DIM), g_send.at[1])
-    drain(halves, w_send.at[0])
-    drain(halves, w_send.at[4])
+    drain(lat.at[:, pl.ds(0, n_tp - 1)])
+    drain(slabs(n_tp - 1, VALUE_DIM))
+    for _ in range(2):
+        drain(halves)
 
     @pl.when(jnp.logical_or(inner, is_near(t)))
     def _():
-        drain(slabs(n_tp - 1, cols), g_send.at[0])
+        drain(slabs(n_tp - 1, cols))
 
     @pl.when(edge)
     def _():
-        drain(lat.at[0, pl.ds(0, 1)], l_send.at[0])
-        drain(halves, w_send.at[3])
+        drain(lat.at[0, pl.ds(0, 1)])
+        drain(halves)
 
     @pl.when(helped)
     def _():
-        lend().wait_send()
+        drain(ql)
 
     @pl.when(helps)
     def _():
-        drain(asked.at[0], q_send.at[0])
-        tell().wait_send()
+        drain(asked.at[0])
+        drain(tally)
 
     @pl.when(inner)
     def _():
-        drain(lat.at[0, pl.ds(0, 2)], l_send.at[0])
-        drain(lat.at[0, pl.ds(0, 3)], l_send.at[1])
-        drain(halves, w_send.at[1])
-        drain(halves, w_send.at[2])
-        drain(wbuf.at[0, pl.ds(0, split), pl.ds(0, half)], w_send.at[5])
-        across_piece().wait_send()
-        drain(wbuf.at[0, 0, pl.ds(0, half + piece)], w_send.at[7])
-        hand(core).wait_send()
-        drain(far_out, f_send.at[0])
+        for count in (2, 3):
+            drain(lat.at[0, pl.ds(0, count)])
+        for _ in range(3):
+            drain(halves)
+        drain(asked.at[0])
+        drain(far_out)
 
     pltpu.make_async_copy(out, out, o_local.at[0]).wait()
 
@@ -796,22 +795,17 @@
             vmem(tiled, bf16),
             vmem(tiled, bf16),
             vmem(tiled, bf16),
-            dma((10,)),
+            dma((4,)),
             dma((2,)),
             dma((1,)),
-            dma((3,)),
+            dma((1,)),
             dma((n_sp + 1,)),
             dma((2,)),
-            dma((2,)),
-            dma((8,)),
-            dma((4, TILES)),
+            dma((TILES // 2 + 3 * TILES,)),
             dma((5,)),
             dma((1,)),
-            dma((1,)),
             dma((3,)),
-            dma((3,)),
-            dma((1,)),
-            dma((TILES,)),
+            dma((4,)),
         ],
         compiler_params=pltpu.CompilerParams(
             collective_id=0, has_side_effects=True

time: 39.3 us -> 39.6 us (level)
  no operation moved by 1% of the time
where the time goes in v4:
time: 39.6 us; the launch traced here: 39.4 us
  Pallas kernels  37.7 us (95%)
  local copies, waits for them, and re-layouts  1.67 us (4%)
    pallas_call x1, Pallas kernels, on_device_fused(): pl.pallas_call(functools.partial(kernel, n_sp, n_tp), out_shape=jax.Shape...  37.7 us
    unnamed x1, local copies, waits for them, and re-layouts  1.67 us

profile of v4, /device:TPU:0, one launch (start us, length us, event | category | flops | bytes accessed | tf_op | source)
XLA Modules:
  0.0 39.4 jit_solution(820106533989155449)
XLA Ops:
  0.0 37.7 %shard_map.109 = bf16[128,1024]{1,0:T(8,128)(2,1)} custom-call(bf16[128,768]{1,0:T(8,128)(2,1)} %ql_hbm.1, bf16[32,256]{1,0:T(8,128)(2,1)} %kl.1, bf16[32,64]{1,0:T(8,128)(2,1)} %rk.1, f32[6,128]{1,0:T(8,128)} %bitcast.3, f32[1,256]{1,0:T(1,128)} %bitcast.5, f32[1,512]{1,0:T(1,128)} %bitcast.4, f32[512,128]{1,0:T(8,128)} %constant.2.clone.table_hbm, ...), custom_call_target="tpu_custom_call" | custom-call | tf_op jit(solution)/shard_map/pallas_call | solution.py:767
  37.8 1.7 %copy.13 = bf16[128,1024]{1,0:T(8,128)(2,1)} copy(bf16[128,1024]{1,0:T(8,128)(2,1)} %shard_map.109) | data formatting | bytes 524288

commit v5 on v4

--- a/solution.py
+++ b/solution.py
@@ -133,6 +133,8 @@
 LANES = 128
 LINE = 4
 TILES = 8
+TAILS = (3, 1)
+AT_EXIT = 2
 
 
 def rope_table(tokens, width):
@@ -156,7 +158,7 @@
     ql_hbm, kl, rk, qg_hbm, lg_hbm, og_hbm, table_hbm, qup, kup, vup, ow, out_hbm,
     ql, ql_outer, qg, lg, og, table,
     lat, wbuf, qbuf, kbuf, vbuf, latn, kturn, qfull, qfull_outer, qnorm, gall, squares, squares_outer, tally,
-    acc, asked,
+    acc, far_acc, asked,
     far_out, far_in, out,
     local, w_local, o_local, sends, l_recv, g_recv, w_recv, m_recv, q_recv, h_recv, f_recv,
 ):
@@ -168,7 +170,6 @@
     block_rows = ql.shape[0]
     depth = ow.shape[0]
     half = depth // 2
-    piece = half // 2
     tile = wbuf.shape[3]
     heads = kup.shape[1] // NOPE_DIM
     cols = heads * VALUE_DIM
@@ -282,11 +283,13 @@
 
     FROM_OUTER = 0
     FROM_CENTRE, BEYOND_NEAR, BEYOND_FAR = (TILES // 2 + TILES * i for i in range(3))
-    CENTRE_FAR, TAIL_TILE, TAIL_PIECE, REST_TILES, REST_PIECE = range(5)
-    last, split = TILES - 1, TILES - 2
-
-    def rows_of(b, p, f, start=0, rows=None):
-        return wbuf.at[b, f, pl.ds(pl.multiple_of(p * half + start, piece), rows or half)]
+    CENTRE_FAR, EARLY_TAIL, LATE_TAIL, REST = range(4)
+    last = TILES - 1
+    cut_most, cut_least = TILES - max(TAILS), TILES - min(TAILS)
+    first_tail = [TILES - count for count in TAILS]
+
+    def rows_of(b, p, f):
+        return wbuf.at[b, f, pl.ds(pl.multiple_of(p * half, half), half)]
 
     def moved(ref, recv, target):
         return remote(ref, ref, recv, target)
@@ -310,15 +313,11 @@
     def across_beyond(f):
         return moved(rows_of(beyond, parity, f), w_recv.at[BEYOND_FAR + f], {"grp": partner})
 
-    def across_piece():
-        return moved(
-            rows_of(beyond, parity, split, 0, piece), w_recv.at[BEYOND_FAR + split], {"grp": partner}
-        )
-
-    def pass_tail(f, start=0, rows=None):
-        return moved(
-            rows_of(outer, 1 - parity, f, start, rows), w_recv.at[BEYOND_FAR + f], {"sp": centre}
-        )
+    def pass_tail(f):
+        return moved(rows_of(outer, 1 - parity, f), w_recv.at[BEYOND_FAR + f], {"sp": centre})
+
+    def of_tiles(count):
+        return wbuf.at[0, pl.ds(0, count), pl.ds(0, half)]
 
     def landed(role, f):
         expect(wbuf.at[0, f, pl.ds(0, half)], w_recv.at[role + f])
@@ -339,11 +338,10 @@
     def near_far():
         @pl.when(edge)
         def _():
-            inward_far(rows_of(z, 1 - parity, split, piece, piece), TAIL_PIECE).start()
-            inward_far(rows_of(z, 1 - parity, split, 0, piece), REST_PIECE).start()
-            inward_far(rows_of(z, 1 - parity, last), TAIL_TILE).start()
-            for f in range(split):
-                inward_far(rows_of(z, 1 - parity, f), REST_TILES).start()
+            for f in range(cut_most, TILES):
+                inward_far(rows_of(z, 1 - parity, f), EARLY_TAIL if f < cut_least else LATE_TAIL).start()
+            for f in range(cut_most):
+                inward_far(rows_of(z, 1 - parity, f), REST).start()
 
     def to_partner(f):
         landed(FROM_CENTRE, f)
@@ -370,31 +368,31 @@
 
     def second_hop(f):
         landed(BEYOND_NEAR, f)
-        if f < split:
+        if f < cut_most:
             across_beyond(f).start()
-        if f == split:
-            @pl.when(core == 1)
-            def _():
-                across_piece().start()
-
-    def pass_tails():
-        expect(wbuf.at[0, 0, pl.ds(0, piece)], m_recv.at[TAIL_PIECE])
-        pass_tail(split, piece, piece).start()
-
-        @pl.when(core == 0)
-        def _():
-            expect(wbuf.at[0, 0, pl.ds(0, piece)], m_recv.at[REST_PIECE])
-            pass_tail(split, 0, piece).start()
-
-        expect(wbuf.at[0, 0, pl.ds(0, half)], m_recv.at[TAIL_TILE])
-        pass_tail(last).start()
+        else:
+            for c, first in enumerate(first_tail):
+                if f < first:
+                    @pl.when(core == c)
+                    def _():
+                        across_beyond(f).start()
+
+    def tails(c):
+        @pl.when(core == c)
+        def _():
+            if first_tail[c] == cut_most:
+                expect(of_tiles(cut_least - cut_most), m_recv.at[EARLY_TAIL])
+            expect(of_tiles(TILES - cut_least), m_recv.at[LATE_TAIL])
+            for f in range(first_tail[c], TILES):
+                pass_tail(f).start()
 
     def outer_rest():
-        expect(wbuf.at[0, pl.ds(0, split), pl.ds(0, half)], m_recv.at[REST_TILES])
-
-        @pl.when(core == 1)
-        def _():
-            expect(wbuf.at[0, 0, pl.ds(0, piece)], m_recv.at[REST_PIECE])
+        expect(of_tiles(cut_most), m_recv.at[REST])
+        for c, first in enumerate(first_tail):
+            if first != cut_most:
+                @pl.when(core == c)
+                def _():
+                    expect(of_tiles(cut_least - cut_most), m_recv.at[EARLY_TAIL])
 
     def centre_far():
         expect(wbuf.at[0, :, pl.ds(0, half)], m_recv.at[CENTRE_FAR])
@@ -526,7 +524,7 @@
     def heard():
         hand(1 - core).wait_recv()
 
-    groups = (tuple(range(split - 2)), (split - 2, split - 1), (split,), (last,))
+    groups = (tuple(range(last - 3)), (last - 3, last - 2), (last - 1,), (last,))
 
     def answer(f):
         n = [f in some for some in groups].index(True)
@@ -564,6 +562,7 @@
             call(i)
 
     tiles = range(TILES)
+    late = TILES - far_acc.shape[0]
     pairs = [(f, f + 1) for f in range(0, TILES, 2)]
 
     loads[0].wait()
@@ -584,10 +583,10 @@
     def _():
         lend().start()
 
-    run(near, range(3))
+    run(near, range(AT_EXIT))
     queries()
     arrive(1)
-    run(near, range(3, TILES))
+    run(near, range(AT_EXIT, TILES))
     run(near_out, range(2))
     inner_partner(range(2))
     arrive(2)
@@ -678,33 +677,51 @@
             for f in some:
                 put(f, acc[f] + far_in[f].astype(jnp.float32))
 
+    def part_of(p):
+        return pl.ds(pl.multiple_of(p * half, half), half)
+
+    def half_dot(f, p):
+        return jnp.dot(
+            asked[beyond - far_base, :, part_of(p)], wbuf[beyond, f, part_of(p)],
+            preferred_element_type=jnp.float32,
+        )
+
+    def prepare(f):
+        far_acc[f - late] = half_dot(f, parity) + dot(asked[centre - far_base], centre, (f,))
+
     def reply(f):
         landed(BEYOND_FAR, f)
-        far = dot(asked[beyond - far_base], beyond, (f,)) + dot(asked[centre - far_base], centre, (f,))
+        if f < late:
+            far = dot(asked[beyond - far_base], beyond, (f,)) + dot(asked[centre - far_base], centre, (f,))
+        else:
+            far = far_acc[f - late] + half_dot(f, 1 - parity)
         far_out[f] = far.astype(far_out.dtype)
         answer(f).start()
 
+    def own(some):
+        keep(some, dot(gained(z), z, some) + dot(gained(centre), centre, some), fresh=True)
+
     @pl.when(inner)
     def _():
-        pl.when(core == 0)(pass_tails)
+        tails(0)
         run(second_hop, range(3, 4))
         heard()
         centre_far()
-        for f in range(4):
-            reply(f)
-            if f == 2:
-                pl.when(core == 1)(pass_tails)
-            run(second_hop, range(f + 4, f + 5))
-        reply(4)
+        reply(0)
+        run(second_hop, range(4, 5))
+        reply(1)
+        run(second_hop, range(5, 6))
+        reply(2)
+        tails(1)
+        run(second_hop, range(6, 7))
+        run(prepare, range(late, late + 1))
+        reply(3)
+        run(second_hop, range(7, 8))
+        run(prepare, range(late + 1, TILES))
+        run(reply, range(4, TILES))
         gather()
         set_scale()
-        for some in pairs[:2]:
-            keep(some, dot(gained(z), z, some) + dot(gained(centre), centre, some), fresh=True)
-        reply(5)
-        reply(6)
-        reply(7)
-        for some in pairs[2:]:
-            keep(some, dot(gained(z), z, some) + dot(gained(centre), centre, some), fresh=True)
+        run(own, pairs)
         outer_rest()
         for some in pairs:
             total = dot(gained(outer), outer, some) + dot(gained(beyond), beyond, some)
@@ -791,6 +808,7 @@
             vmem((block_rows, VALUE_DIM), jnp.float32),
             vmem((block_rows, VALUE_DIM), bf16),
             vmem(tiled, jnp.float32),
+            vmem((max(TAILS), *tiled[1:]), jnp.float32),
             vmem((n_tp // 2, block_rows, cols), bf16),
             vmem(tiled, bf16),
             vmem(tiled, bf16),
@@ -802,7 +820,7 @@
             dma((n_sp + 1,)),
             dma((2,)),
             dma((TILES // 2 + 3 * TILES,)),
-            dma((5,)),
+            dma((4,)),
             dma((1,)),
             dma((3,)),
             dma((4,)),

time: 39.6 us -> 38.6 us (0.975)
  Pallas kernels: 37.7 us -> 36.8 us
    pallas_call x1, Pallas kernels: 37.7 us -> 36.8 us  [on_device_fused(): pl.pallas_call(functools.partial(kernel, n_sp, n_tp), out_shape=jax.Shape...]
where the time goes in v5:
time: 38.6 us; the launch traced here: 38.5 us
  Pallas kernels  36.8 us (95%)
  local copies, waits for them, and re-layouts  1.67 us (4%)
    pallas_call x1, Pallas kernels, on_device_fused(): pl.pallas_call(functools.partial(kernel, n_sp, n_tp), out_shape=jax.Shape...  36.8 us
    unnamed x1, local copies, waits for them, and re-layouts  1.67 us

profile of v5, /device:TPU:0, one launch (start us, length us, event | category | flops | bytes accessed | tf_op | source)
XLA Modules:
  0.0 38.5 jit_solution(16245380336319431796)
XLA Ops:
  0.0 36.8 %shard_map.109 = bf16[128,1024]{1,0:T(8,128)(2,1)} custom-call(bf16[128,768]{1,0:T(8,128)(2,1)} %ql_hbm.1, bf16[32,256]{1,0:T(8,128)(2,1)} %kl.1, bf16[32,64]{1,0:T(8,128)(2,1)} %rk.1, f32[6,128]{1,0:T(8,128)} %bitcast.3, f32[1,256]{1,0:T(1,128)} %bitcast.5, f32[1,512]{1,0:T(1,128)} %bitcast.4, f32[512,128]{1,0:T(8,128)} %constant.2.clone.table_hbm, ...), custom_call_target="tpu_custom_call" | custom-call | tf_op jit(solution)/shard_map/pallas_call | solution.py:784
  36.8 1.7 %copy.13 = bf16[128,1024]{1,0:T(8,128)(2,1)} copy(bf16[128,1024]{1,0:T(8,128)(2,1)} %shard_map.109) | data formatting | bytes 524288

commit v6 on v5

--- a/solution.py
+++ b/solution.py
@@ -155,12 +155,12 @@
 
 def kernel(
     n_sp, n_tp,
-    ql_hbm, kl, rk, qg_hbm, lg_hbm, og_hbm, table_hbm, qup, kup, vup, ow, out_hbm,
+    ql_hbm, kl, rk, qg_hbm, lg_hbm, og_hbm, table_hbm, qup, kup, vup, ow, out,
     ql, ql_outer, qg, lg, og, table,
     lat, wbuf, qbuf, kbuf, vbuf, latn, kturn, qfull, qfull_outer, qnorm, gall, squares, squares_outer, tally,
     acc, far_acc, asked,
-    far_out, far_in, out,
-    local, w_local, o_local, sends, l_recv, g_recv, w_recv, m_recv, q_recv, h_recv, f_recv,
+    far_out, far_in,
+    local, w_local, sends, l_recv, g_recv, w_recv, m_recv, q_recv, h_recv, f_recv,
 ):
     z, t, g = lax.axis_index("sp"), lax.axis_index("tp"), lax.axis_index("grp")
     parity = lax.rem(g, 2)
@@ -544,9 +544,6 @@
             part = total[:, n * tile : (n + 1) * tile]
             acc[f] = part if fresh else acc[f] + part
 
-    def stored(f):
-        return pltpu.make_async_copy(out.at[f], out_hbm.at[:, pl.ds(f * tile, tile)], o_local.at[0])
-
     def set_scale():
         square = gall[0, :, cols : cols + 1].astype(jnp.float32)
         for p in range(1, n_tp):
@@ -554,8 +551,7 @@
         squares[...] = jnp.broadcast_to(lax.rsqrt(square / (n_tp * cols) + norm_eps), squares.shape)
 
     def put(f, total):
-        out[f] = (total * squares[...]).astype(out.dtype)
-        stored(f).start()
+        out[:, f * tile : (f + 1) * tile] = (total * squares[...]).astype(out.dtype)
 
     def run(call, some):
         for i in some:
@@ -652,9 +648,8 @@
 
         @pl.when(inner)
         def _():
-            run(second_hop, range(2))
+            run(second_hop, range(3))
             hand_on()
-            run(second_hop, range(2, 3))
 
     @pl.when(helped)
     def _():
@@ -703,12 +698,12 @@
 
     @pl.when(inner)
     def _():
-        tails(0)
         run(second_hop, range(3, 4))
         heard()
         centre_far()
         reply(0)
         run(second_hop, range(4, 5))
+        tails(0)
         reply(1)
         run(second_hop, range(5, 6))
         reply(2)
@@ -761,8 +756,6 @@
         drain(asked.at[0])
         drain(far_out)
 
-    pltpu.make_async_copy(out, out, o_local.at[0]).wait()
-
 
 MESH = pl.DeviceIdType.MESH
 
@@ -783,9 +776,9 @@
     in_hbm = pl.BlockSpec(memory_space=pl.ANY)
     return pl.pallas_call(
         functools.partial(kernel, n_sp, n_tp),
-        out_shape=jax.ShapeDtypeStruct((block_rows, features), bf16),
+        out_shape=vmem((block_rows, features), bf16),
         in_specs=[in_hbm] * 11,
-        out_specs=in_hbm,
+        out_specs=pl.BlockSpec(memory_space=pltpu.VMEM),
         scratch_shapes=[
             vmem(query_latent.shape, bf16),
             vmem(query_latent.shape, bf16),
@@ -812,10 +805,8 @@
             vmem((n_tp // 2, block_rows, cols), bf16),
             vmem(tiled, bf16),
             vmem(tiled, bf16),
-            vmem(tiled, bf16),
             dma((4,)),
             dma((2,)),
-            dma((1,)),
             dma((1,)),
             dma((n_sp + 1,)),
             dma((2,)),

time: 38.6 us -> 37 us (0.959)
  local copies, waits for them, and re-layouts: 1.67 us -> 0.71 us
  Pallas kernels: 36.8 us -> 36.2 us
    unnamed x1, local copies, waits for them, and re-layouts: 1.67 us -> 0.71 us
    pallas_call x1, Pallas kernels: 36.8 us -> 36.2 us  [on_device_fused(): pl.pallas_call(functools.partial(kernel, n_sp, n_tp), out_shape=vmem((blo...]
where the time goes in v6:
time: 37 us; the launch traced here: 36.9 us
  Pallas kernels  36.2 us (98%)
  local copies, waits for them, and re-layouts  0.71 us (2%)
    pallas_call x1, Pallas kernels, on_device_fused(): pl.pallas_call(functools.partial(kernel, n_sp, n_tp), out_shape=vmem((blo...  36.2 us

profile of v6, /device:TPU:0, one launch (start us, length us, event | category | flops | bytes accessed | tf_op | source)
XLA Modules:
  0.0 36.9 jit_solution(5447490556296280299)
XLA Ops:
  0.0 36.2 %shard_map.109 = bf16[128,1024]{1,0:T(8,128)(2,1)S(1)} custom-call(bf16[128,768]{1,0:T(8,128)(2,1)} %ql_hbm.1, bf16[32,256]{1,0:T(8,128)(2,1)} %kl.1, bf16[32,64]{1,0:T(8,128)(2,1)} %rk.1, f32[6,128]{1,0:T(8,128)} %bitcast.3, f32[1,256]{1,0:T(1,128)} %bitcast.5, f32[1,512]{1,0:T(1,128)} %bitcast.4, f32[512,128]{1,0:T(8,128)} %constant.2.clone.table_hbm, ...), custom_call_target="tpu_custom_call" | custom-call | tf_op jit(solution)/shard_map/pallas_call | solution.py:777
  36.2 0.7 %copy.13 = bf16[128,1024]{1,0:T(8,128)(2,1)} copy(bf16[128,1024]{1,0:T(8,128)(2,1)S(1)} %shard_map.109) | data formatting | bytes 524288

commit v7 on v6

--- a/solution.py
+++ b/solution.py
@@ -133,8 +133,10 @@
 LANES = 128
 LINE = 4
 TILES = 8
-TAILS = (3, 1)
-AT_EXIT = 2
+TAILS = (2, 2)
+AT_EXIT = (3, 1)
+ORDERS = ((4, 6, 5, 7), (4, 5, 6, 7))
+LATE = 3
 
 
 def rope_table(tokens, width):
@@ -281,7 +283,7 @@
 
             spread(z + d)
 
-    FROM_OUTER = 0
+    FROM_OUTER, SECOND_PIECE = 0, TILES // 2 + 3 * TILES
     FROM_CENTRE, BEYOND_NEAR, BEYOND_FAR = (TILES // 2 + TILES * i for i in range(3))
     CENTRE_FAR, EARLY_TAIL, LATE_TAIL, REST = range(4)
     last = TILES - 1
@@ -294,12 +296,23 @@
     def moved(ref, recv, target):
         return remote(ref, ref, recv, target)
 
+    def pieces(b, f):
+        if f:
+            return [(rows_of(b, parity, f), FROM_CENTRE + f)]
+        rows = half // 2
+        return [
+            (wbuf.at[b, f, pl.ds(pl.multiple_of(parity * half + n * rows, rows), rows)], role)
+            for n, role in enumerate((FROM_CENTRE, SECOND_PIECE))
+        ]
+
     def inward(f):
-        role = jnp.where(edge, FROM_OUTER + f // 2, FROM_CENTRE + f)
-        return moved(rows_of(z, parity, f), w_recv.at[role], {"sp": centre})
+        return [
+            moved(ref, w_recv.at[jnp.where(edge, FROM_OUTER + f // 2, role)], {"sp": centre})
+            for ref, role in pieces(z, f)
+        ]
 
     def outward(f):
-        return moved(rows_of(z, parity, f), w_recv.at[FROM_CENTRE + f], {"sp": outer})
+        return [moved(ref, w_recv.at[role], {"sp": outer}) for ref, role in pieces(z, f)]
 
     def passed(f):
         return moved(rows_of(outer, parity, f), w_recv.at[BEYOND_NEAR + f], {"sp": centre})
@@ -307,8 +320,6 @@
     def inward_far(ref, part):
         return moved(ref, m_recv.at[part], {"sp": centre})
 
-    def across(f):
-        return moved(rows_of(centre, parity, f), m_recv.at[CENTRE_FAR], {"grp": partner})
 
     def across_beyond(f):
         return moved(rows_of(beyond, parity, f), w_recv.at[BEYOND_FAR + f], {"grp": partner})
@@ -328,12 +339,14 @@
         if f == 1:
             rest = wbuf.at[z, pl.ds(1, last)]
             pltpu.make_async_copy(rest, rest, w_local.at[1]).wait()
-        inward(f).start()
+        for copy in inward(f):
+            copy.start()
 
     def near_out(f):
         @pl.when(inner)
         def _():
-            outward(f).start()
+            for copy in outward(f):
+                copy.start()
 
     def near_far():
         @pl.when(edge)
@@ -344,8 +357,9 @@
                 inward_far(rows_of(z, 1 - parity, f), REST).start()
 
     def to_partner(f):
-        landed(FROM_CENTRE, f)
-        across(f).start()
+        for ref, role in pieces(centre, f):
+            expect(ref, w_recv.at[role])
+            moved(ref, m_recv.at[CENTRE_FAR], {"grp": partner}).start()
 
     def inner_partner(some):
         @pl.when(inner)
@@ -380,10 +394,12 @@
     def tails(c):
         @pl.when(core == c)
         def _():
-            if first_tail[c] == cut_most:
+            if first_tail[c] < cut_least:
                 expect(of_tiles(cut_least - cut_most), m_recv.at[EARLY_TAIL])
+                for f in range(cut_most, cut_least):
+                    pass_tail(f).start()
             expect(of_tiles(TILES - cut_least), m_recv.at[LATE_TAIL])
-            for f in range(first_tail[c], TILES):
+            for f in range(cut_least, TILES):
                 pass_tail(f).start()
 
     def outer_rest():
@@ -406,8 +422,23 @@
             jnp.bfloat16
         )
 
+    lent_rows = block_rows // 2
+
+    def lent(c):
+        return pl.ds(pl.multiple_of(c * lent_rows, lent_rows), lent_rows)
+
     def lend():
-        return remote(ql, ql_outer, h_recv.at[1], {"sp": centre})
+        return remote(ql.at[lent(core)], ql_outer.at[lent(core)], h_recv.at[1], {"sp": centre})
+
+    def swap(c):
+        part = ql_outer.at[lent(c)]
+        return remote(part, part, h_recv.at[3], {"tp": sibling})
+
+    def lend_on():
+        @pl.when(helps)
+        def _():
+            lend().wait_recv()
+            swap(core).start()
 
     def queries():
         for load in loads[3:5]:
@@ -417,7 +448,7 @@
     def outer_queries():
         @pl.when(helps)
         def _():
-            lend().wait_recv()
+            swap(1 - core).wait_recv()
             project(ql_outer, qfull_outer)
 
     def latents():
@@ -524,11 +555,10 @@
     def heard():
         hand(1 - core).wait_recv()
 
-    groups = (tuple(range(last - 3)), (last - 3, last - 2), (last - 1,), (last,))
+    early = TILES - LATE
 
     def answer(f):
-        n = [f in some for some in groups].index(True)
-        return remote(far_out.at[f], far_in.at[f], f_recv.at[n], {"sp": outer})
+        return remote(far_out.at[f], far_in.at[f], f_recv.at[max(0, f - early + 1)], {"sp": outer})
 
     def wide_of(b, some):
         return jnp.concatenate([wbuf[b, f] for f in some], axis=1)
@@ -558,7 +588,6 @@
             call(i)
 
     tiles = range(TILES)
-    late = TILES - far_acc.shape[0]
     pairs = [(f, f + 1) for f in range(0, TILES, 2)]
 
     loads[0].wait()
@@ -579,15 +608,20 @@
     def _():
         lend().start()
 
-    run(near, range(AT_EXIT))
+    for c, count in enumerate(AT_EXIT):
+        pl.when(core == c)(functools.partial(run, near, range(count)))
     queries()
     arrive(1)
-    run(near, range(AT_EXIT, TILES))
+    for c, count in enumerate(AT_EXIT):
+        pl.when(core == c)(functools.partial(run, near, range(count, TILES)))
     run(near_out, range(2))
-    inner_partner(range(2))
+    for c, count in enumerate(AT_EXIT):
+        pl.when(core == c)(functools.partial(inner_partner, range(max(count, 2))))
+    lend_on()
     arrive(2)
     run(near_out, range(2, TILES))
-    inner_partner(range(2, 3))
+    for c, count in enumerate(AT_EXIT):
+        pl.when(core == c)(functools.partial(inner_partner, range(max(count, 2), 3)))
     arrive(3)
     near_far()
     outer_queries()
@@ -667,10 +701,18 @@
         centre_far()
         for some in pairs:
             keep(some, dot(gained(centre), centre, some))
-        for n, some in enumerate(groups):
-            expect(far_in.at[pl.ds(0, len(some))], f_recv.at[n])
-            for f in some:
-                put(f, acc[f] + far_in[f].astype(jnp.float32))
+        def add(f):
+            put(f, acc[f] + far_in[f].astype(jnp.float32))
+
+        expect(far_in.at[pl.ds(0, early)], f_recv.at[0])
+        run(add, range(early))
+        for c, order in enumerate(ORDERS):
+            @pl.when(core == c)
+            def _():
+                for f in order:
+                    if f >= early:
+                        expect(far_in.at[0], f_recv.at[f - early + 1])
+                        add(f)
 
     def part_of(p):
         return pl.ds(pl.multiple_of(p * half, half), half)
@@ -682,14 +724,14 @@
         )
 
     def prepare(f):
-        far_acc[f - late] = half_dot(f, parity) + dot(asked[centre - far_base], centre, (f,))
+        far_acc[f - early] = half_dot(f, parity) + dot(asked[centre - far_base], centre, (f,))
 
     def reply(f):
         landed(BEYOND_FAR, f)
-        if f < late:
+        if f < early:
             far = dot(asked[beyond - far_base], beyond, (f,)) + dot(asked[centre - far_base], centre, (f,))
         else:
-            far = far_acc[f - late] + half_dot(f, 1 - parity)
+            far = far_acc[f - early] + half_dot(f, 1 - parity)
         far_out[f] = far.astype(far_out.dtype)
         answer(f).start()
 
@@ -709,11 +751,11 @@
         reply(2)
         tails(1)
         run(second_hop, range(6, 7))
-        run(prepare, range(late, late + 1))
         reply(3)
         run(second_hop, range(7, 8))
-        run(prepare, range(late + 1, TILES))
-        run(reply, range(4, TILES))
+        run(prepare, range(early, TILES))
+        for c, order in enumerate(ORDERS):
+            pl.when(core == c)(functools.partial(run, reply, order))
         gather()
         set_scale()
         run(own, pairs)
@@ -740,12 +782,13 @@
 
     @pl.when(helped)
     def _():
-        drain(ql)
+        drain(ql.at[pl.ds(0, lent_rows)])
 
     @pl.when(helps)
     def _():
         drain(asked.at[0])
         drain(tally)
+        drain(ql.at[pl.ds(0, lent_rows)])
 
     @pl.when(inner)
     def _():
@@ -801,7 +844,7 @@
             vmem((block_rows, VALUE_DIM), jnp.float32),
             vmem((block_rows, VALUE_DIM), bf16),
             vmem(tiled, jnp.float32),
-            vmem((max(TAILS), *tiled[1:]), jnp.float32),
+            vmem((LATE, *tiled[1:]), jnp.float32),
             vmem((n_tp // 2, block_rows, cols), bf16),
             vmem(tiled, bf16),
             vmem(tiled, bf16),
@@ -810,10 +853,10 @@
             dma((1,)),
             dma((n_sp + 1,)),
             dma((2,)),
-            dma((TILES // 2 + 3 * TILES,)),
+            dma((TILES // 2 + 3 * TILES + 1,)),
             dma((4,)),
             dma((1,)),
-            dma((3,)),
+            dma((4,)),
             dma((4,)),
         ],
         compiler_params=pltpu.CompilerParams(

time: 37 us -> 36.9 us (level)
  no operation moved by 1% of the time
where the time goes in v7:
time: 36.9 us; the launch traced here: 36.7 us
  Pallas kernels  36 us (98%)
  local copies, waits for them, and re-layouts  0.71 us (2%)
    pallas_call x1, Pallas kernels, on_device_fused(): pl.pallas_call(functools.partial(kernel, n_sp, n_tp), out_shape=vmem((blo...  36 us

profile of v7, /device:TPU:0, one launch (start us, length us, event | category | flops | bytes accessed | tf_op | source)
XLA Modules:
  0.0 36.7 jit_solution(5537578332765272581)
XLA Ops:
  0.0 36.0 %shard_map.109 = bf16[128,1024]{1,0:T(8,128)(2,1)S(1)} custom-call(bf16[128,768]{1,0:T(8,128)(2,1)} %ql_hbm.1, bf16[32,256]{1,0:T(8,128)(2,1)} %kl.1, bf16[32,64]{1,0:T(8,128)(2,1)} %rk.1, f32[6,128]{1,0:T(8,128)} %bitcast.3, f32[1,256]{1,0:T(1,128)} %bitcast.5, f32[1,512]{1,0:T(1,128)} %bitcast.4, f32[512,128]{1,0:T(8,128)} %constant.2.clone.table_hbm, ...), custom_call_target="tpu_custom_call" | custom-call | tf_op jit(solution)/shard_map/pallas_call | solution.py:820
  36.0 0.7 %copy.13 = bf16[128,1024]{1,0:T(8,128)(2,1)} copy(bf16[128,1024]{1,0:T(8,128)(2,1)S(1)} %shard_map.109) | data formatting | bytes 524288

commit v8 on v7

--- a/solution.py
+++ b/solution.py
@@ -692,6 +692,41 @@
 
     share(heads)
 
+    def drain_all():
+        halves = wbuf.at[0, :, pl.ds(0, half)]
+        drain(lat.at[:, pl.ds(0, n_tp - 1)])
+        drain(slabs(n_tp - 1, VALUE_DIM))
+        for _ in range(2):
+            drain(halves)
+
+        @pl.when(jnp.logical_or(inner, is_near(t)))
+        def _():
+            drain(slabs(n_tp - 1, cols))
+
+        @pl.when(edge)
+        def _():
+            drain(lat.at[0, pl.ds(0, 1)])
+            drain(halves)
+
+        @pl.when(helped)
+        def _():
+            drain(ql.at[pl.ds(0, lent_rows)])
+
+        @pl.when(helps)
+        def _():
+            drain(asked.at[0])
+            drain(tally)
+            drain(ql.at[pl.ds(0, lent_rows)])
+
+        @pl.when(inner)
+        def _():
+            for count in (2, 3):
+                drain(lat.at[0, pl.ds(0, count)])
+            for _ in range(3):
+                drain(halves)
+            drain(asked.at[0])
+            drain(far_out)
+
     @pl.when(edge)
     def _():
         gather()
@@ -704,6 +739,7 @@
         def add(f):
             put(f, acc[f] + far_in[f].astype(jnp.float32))
 
+        drain_all()
         expect(far_in.at[pl.ds(0, early)], f_recv.at[0])
         run(add, range(early))
         for c, order in enumerate(ORDERS):
@@ -765,39 +801,7 @@
             for n, f in enumerate(some):
                 put(f, acc[f] + total[:, n * tile : (n + 1) * tile])
 
-    halves = wbuf.at[0, :, pl.ds(0, half)]
-    drain(lat.at[:, pl.ds(0, n_tp - 1)])
-    drain(slabs(n_tp - 1, VALUE_DIM))
-    for _ in range(2):
-        drain(halves)
-
-    @pl.when(jnp.logical_or(inner, is_near(t)))
-    def _():
-        drain(slabs(n_tp - 1, cols))
-
-    @pl.when(edge)
-    def _():
-        drain(lat.at[0, pl.ds(0, 1)])
-        drain(halves)
-
-    @pl.when(helped)
-    def _():
-        drain(ql.at[pl.ds(0, lent_rows)])
-
-    @pl.when(helps)
-    def _():
-        drain(asked.at[0])
-        drain(tally)
-        drain(ql.at[pl.ds(0, lent_rows)])
-
-    @pl.when(inner)
-    def _():
-        for count in (2, 3):
-            drain(lat.at[0, pl.ds(0, count)])
-        for _ in range(3):
-            drain(halves)
-        drain(asked.at[0])
-        drain(far_out)
+    pl.when(inner)(drain_all)
 
 
 MESH = pl.DeviceIdType.MESH

time: 36.9 us -> 36.9 us (level)
  no operation moved by 1% of the time
where the time goes in v8:
time: 36.9 us; the launch traced here: 36.7 us
  Pallas kernels  36 us (98%)
  local copies, waits for them, and re-layouts  0.71 us (2%)
    pallas_call x1, Pallas kernels, on_device_fused(): pl.pallas_call(functools.partial(kernel, n_sp, n_tp), out_shape=vmem((blo...  36 us

profile of v8, /device:TPU:0, one launch (start us, length us, event | category | flops | bytes accessed | tf_op | source)
XLA Modules:
  0.0 36.7 jit_solution(12098667463598962819)
XLA Ops:
  0.0 36.0 %shard_map.109 = bf16[128,1024]{1,0:T(8,128)(2,1)S(1)} custom-call(bf16[128,768]{1,0:T(8,128)(2,1)} %ql_hbm.1, bf16[32,256]{1,0:T(8,128)(2,1)} %kl.1, bf16[32,64]{1,0:T(8,128)(2,1)} %rk.1, f32[6,128]{1,0:T(8,128)} %bitcast.3, f32[1,256]{1,0:T(1,128)} %bitcast.5, f32[1,512]{1,0:T(1,128)} %bitcast.4, f32[512,128]{1,0:T(8,128)} %constant.2.clone.table_hbm, ...), custom_call_target="tpu_custom_call" | custom-call | tf_op jit(solution)/shard_map/pallas_call | solution.py:824
  36.0 0.7 %copy.13 = bf16[128,1024]{1,0:T(8,128)(2,1)} copy(bf16[128,1024]{1,0:T(8,128)(2,1)S(1)} %shard_map.109) | data formatting | bytes 524288
